TPU v7x, 256 devices: a 4x2x16 block of a 4x16x16 slice. The times are simulated.
256 devices in a mesh: grp: 2 (over y), sp: 16 (over z), fs: 4 (over x), tp: 2 (over core).
Axes of the slice: x: 4, y: 2, z: 16, core: 2. Of those that a mesh axis runs over, the one named last changes fastest.
The devices are a block of a 4x16x16 slice.
Arguments:
- tokens: bfloat16 [8, 2048, 2048], P(('grp', 'fs'), 'sp', 'tp'), parts along dimension 0, may hold values from -6 to 6
- norm_gain: float32 [2048], replicated, may hold values from 0.1 to 1.9
- w_z: bfloat16 [2048, 2048], P(('sp', 'fs'), 'tp'), may hold values from -0.125 to 0.125
- w_x: bfloat16 [2048, 2048], P(('sp', 'fs'), 'tp'), may hold values from -0.125 to 0.125
- w_b: bfloat16 [2048, 512], P(('sp', 'fs'), 'tp'), may hold values from -0.125 to 0.125
- w_c: bfloat16 [2048, 512], P(('sp', 'fs'), 'tp'), may hold values from -0.125 to 0.125
- w_dt: bfloat16 [2048, 32], P(None, 'tp'), may hold values from -0.125 to 0.125
- w_gate: bfloat16 [2048, 2, 32], P(None, None, 'tp'), may hold values from -0.125 to 0.125
- w_scb: bfloat16 [2048, 2048], P(('sp', 'fs'), 'tp'), may hold values from -0.125 to 0.125
- w_scc: bfloat16 [2048, 2048], P(('sp', 'fs'), 'tp'), may hold values from -0.125 to 0.125
- w_scx: bfloat16 [2048, 2048], P(('sp', 'fs'), 'tp'), may hold values from -0.125 to 0.125
- conv_x: float32 [4, 2048], P(None, 'tp'), may hold values from -3 to 3
- conv_b: float32 [4, 512], P(None, 'tp'), may hold values from -3 to 3
- conv_c: float32 [4, 512], P(None, 'tp'), may hold values from -3 to 3
- conv_sc: float32 [3, 2048], P(None, 'tp'), may hold values from -8 to 8
- dt_bias: float32 [32], P('tp'), may hold values from -1 to 1
- decay_log: float32 [32], P('tp'), as said below
- group_gain: float32 [2048], P('tp'), may hold values from 0.1 to 1.9
- span_shift: float32 [8, 32], P(('grp', 'fs'), 'sp'), parts along dimension 0, may hold values from -1.5 to 1.5
- w_out: bfloat16 [2048, 2048], P(('sp', 'fs'), 'tp'), may hold values from -0.125 to 0.125
Outputs:
- mixed: bfloat16 [8, 2048, 2048], P(('grp', 'fs'), ('sp', 'tp')), parts along dimension 0
There are 2 independent parts, one for each index of `grp`. A program takes and returns all parts, laid end to end along the dimension named above; an argument that names none is the same for every part. Nothing has to cross between parts.
Inputs may be any that keep to these rules, and one draw needn't show every extreme that they name: `decay_log`: one value a head.
All inputs are finite; a program needn't handle non-finite values.
Results may differ from a plain program's by a relative error of at most 0.014.
Values may be sent and summed in bfloat16 or wider, within the bound.
No kernel may reach another device: no remote copies, remote signals or barrier semaphores. Data moves between devices by JAX's collectives and lax.ppermute only.
A program may use at most 128 MiB of HBM per device.

v0:
```python
import jax
import jax.numpy as jnp
from jax import lax
from jax.sharding import PartitionSpec as P

HEAD_DIM = 64
STATE = 64
BLOCK = 64


EPS = 1.0
HIGH = lax.Precision.HIGHEST


def in_order(parts, dim):
    parts = jnp.moveaxis(parts, 0, dim)
    lengths = parts.shape
    return parts.reshape(*lengths[:dim], lengths[dim] * lengths[dim + 1], *lengths[dim + 2 :])


def sent_to_all(x, axis):
    copies = jnp.broadcast_to(x, (lax.axis_size(axis), *x.shape))
    return lax.all_to_all(copies, axis, split_axis=0, concat_axis=0, tiled=True)


def gather_directly(x, axis, dim):
    return in_order(sent_to_all(x, axis), dim)


def in_one_piece(arrays, axis, dim, along):
    widths = [a.shape[along] for a in arrays]
    both = jnp.concatenate(arrays, axis=along)
    filled = lax.all_gather(both, axis, axis=dim, tiled=True)
    return tuple(jnp.split(filled, [sum(widths[:k]) for k in range(1, len(widths))], axis=along))


def sent_together(arrays, axis, split_dim, concat_dim, along):
    widths = [a.shape[along] for a in arrays]
    both = jnp.concatenate(arrays, axis=along)
    filled = lax.all_to_all(both, axis, split_axis=split_dim, concat_axis=concat_dim, tiled=True)
    return tuple(jnp.split(filled, [sum(widths[:k]) for k in range(1, len(widths))], axis=along))


def from_behind(block, axis, distance):
    devices = range(lax.axis_size(axis))
    route = [(i - distance, i) for i in devices if i - distance in devices]
    return lax.ppermute(block, axis, route)


def carried_in(x, axis, combine, identity):
    size, here = (lax.axis_size(axis), lax.axis_index(axis))
    everything = jax.tree.map(
        lambda part, kind: lax.all_gather(part.astype(kind), axis), x, (jnp.bfloat16, jnp.bfloat16)
    )
    start = jax.tree.map(
        lambda part, zero: jnp.broadcast_to(jnp.asarray(zero, part.dtype), part.shape), x, identity
    )

    def hop(k, before):
        reached = k < here
        new = combine(
            before, jax.tree.map(lambda part, own: part[k].astype(own.dtype), everything, x)
        )
        return jax.tree.map(lambda a, b: jnp.where(reached, a, b), new, before)

    return lax.fori_loop(0, size, hop, start)


def gathered_by_axis(x, axes, dim):
    for axis in reversed(axes):
        x = lax.all_gather(x, axis, axis=dim, tiled=True)
    return x


def split_up(x, dim, size):
    before, after = (x.shape[:dim], x.shape[dim + 1 :])
    return jnp.moveaxis(x.reshape(*before, size, -1, *after), dim, 0)


def sent_and_summed(x, axis, dim):
    parts = split_up(x, dim, lax.axis_size(axis))
    arrived = lax.all_to_all(parts, axis, split_axis=0, concat_axis=0, tiled=True)
    return arrived.astype(jnp.float32).sum(axis=0)


def causal_taps(extended, taps):
    width = taps.shape[0]
    length = extended.shape[0] - width + 1
    result = extended[0:length] * taps[0]
    for step in range(1, width):
        result = result + extended[step : step + length] * taps[step]
    return result


def body(
    tokens,
    norm_gain,
    w_z,
    w_x,
    w_b,
    w_c,
    w_dt,
    w_gate,
    w_scb,
    w_scc,
    w_scx,
    conv_x,
    conv_b,
    conv_c,
    conv_sc,
    dt_bias,
    decay_log,
    group_gain,
    span_shift,
    w_out,
):
    whole = gather_directly(tokens[0], "tp", 1)
    rows = whole.astype(jnp.float32)
    inverse_rms = lax.rsqrt(jnp.mean(rows * rows, axis=1, keepdims=True) + EPS)
    normed = (rows * inverse_rms * norm_gain).astype(jnp.bfloat16)
    length = normed.shape[0]
    quarters = (
        lax.all_to_all(w_z, "fs", split_axis=1, concat_axis=0, tiled=True),
        lax.all_to_all(w_x, "fs", split_axis=1, concat_axis=0, tiled=True),
        lax.all_to_all(w_b, "fs", split_axis=1, concat_axis=0, tiled=True),
        lax.all_to_all(w_c, "fs", split_axis=1, concat_axis=0, tiled=True),
        lax.all_to_all(w_scb, "fs", split_axis=1, concat_axis=0, tiled=True),
        lax.all_to_all(w_scc, "fs", split_axis=1, concat_axis=0, tiled=True),
        lax.all_to_all(w_scx, "fs", split_axis=1, concat_axis=0, tiled=True),
    )
    everyone = lax.all_gather(normed[None], "fs", axis=0, tiled=True)
    stacked = everyone.reshape(-1, everyone.shape[2])
    full = in_one_piece(
        (quarters[0], quarters[1], quarters[2], quarters[3], quarters[4], quarters[5], quarters[6]),
        "sp",
        0,
        1,
    )
    shaped = [
        jnp.dot(stacked, weight, preferred_element_type=jnp.float32)
        .astype(jnp.bfloat16)
        .reshape(everyone.shape[0], length, -1)
        for weight in full
    ]
    z_part, x_part, b_part, c_part, scb_part, scc_part, scx_part = shaped
    back = (
        *sent_together((z_part, x_part), "fs", 0, 2, 1),
        *sent_together((b_part, c_part), "fs", 0, 2, 1),
        *sent_together((scb_part, scc_part, scx_part), "fs", 0, 2, 1),
    )
    streams = tuple((member[0] for member in back))
    z_stream, x_stream, b_stream, c_stream, scb_stream, scc_stream, scx_stream = streams
    dt_pre = jnp.dot(normed, w_dt, preferred_element_type=jnp.float32)
    gate_pre = jnp.dot(
        normed, w_gate.reshape(w_gate.shape[0], -1), preferred_element_type=jnp.float32
    ).reshape(length, 2, -1)
    edge = conv_x.shape[0] - 1
    tail_x, tail_b, tail_c, tail_scc, tail_scx = from_behind(
        (
            x_stream[-edge:],
            b_stream[-edge:],
            c_stream[-edge:],
            scc_stream[-edge:],
            scx_stream[-edge:],
        ),
        "sp",
        1,
    )
    x_conv = jax.nn.silu(
        causal_taps(jnp.concatenate([tail_x, x_stream], 0).astype(jnp.float32), conv_x)
    )
    b_conv = jax.nn.silu(
        causal_taps(jnp.concatenate([tail_b, b_stream], 0).astype(jnp.float32), conv_b)
    )
    c_conv = jax.nn.silu(
        causal_taps(jnp.concatenate([tail_c, c_stream], 0).astype(jnp.float32), conv_c)
    )
    sc_width = conv_sc.shape[0]
    short_in = jnp.concatenate([tail_scc, scc_stream], 0).astype(jnp.float32) * jnp.concatenate(
        [tail_scx, scx_stream], 0
    ).astype(jnp.float32)
    short_out = scb_stream.astype(jnp.float32) * causal_taps(
        short_in[edge - sc_width + 1 :], conv_sc
    )
    heads = dt_bias.shape[0]
    groups = b_conv.shape[1] // STATE
    blocks = length // BLOCK
    shift = jnp.repeat(span_shift[0], BLOCK)[:, None]
    step_size = jax.nn.softplus(dt_pre + dt_bias + shift)
    rate = -jnp.exp(decay_log)
    x_heads = x_conv.reshape(blocks, BLOCK, heads, HEAD_DIM)
    b_heads = jnp.repeat(b_conv.reshape(blocks, BLOCK, groups, STATE), heads // groups, axis=2)
    c_heads = jnp.repeat(c_conv.reshape(blocks, BLOCK, groups, STATE), heads // groups, axis=2)
    step_blocks = step_size.reshape(blocks, BLOCK, heads)
    cum_log = jnp.cumsum(step_blocks * rate, axis=1)
    lower = lax.iota(jnp.int32, BLOCK)[:, None] >= lax.iota(jnp.int32, BLOCK)[None, :]
    log_gap = cum_log[:, :, None, :] - cum_log[:, None, :, :]
    pair_decay = jnp.where(lower[None, :, :, None], jnp.exp(jnp.minimum(log_gap, 0.0)), 0.0)
    scores = jnp.einsum("cihn,cjhn->cijh", c_heads, b_heads, precision=HIGH)
    x_step = x_heads * step_blocks[..., None]
    inner = jnp.einsum("cijh,cjhp->cihp", scores * pair_decay, x_step, precision=HIGH)
    to_end = jnp.exp(cum_log[:, -1:, :] - cum_log)
    fresh = jnp.einsum("cjhn,cjhp->chpn", b_heads * to_end[..., None], x_step, precision=HIGH)
    block_log = cum_log[:, -1, :]

    def advance(state, item):
        fresh_block, log_block = item
        return (state * jnp.exp(log_block)[:, None, None] + fresh_block, state)

    final_state, entering = lax.scan(
        advance, jnp.zeros(fresh.shape[1:], jnp.float32), (fresh, block_log)
    )
    lead_log = jnp.cumsum(block_log, axis=0) - block_log
    total_log = jnp.sum(block_log, axis=0)
    flat_state = final_state.reshape(heads, -1)

    def combine(earlier, later):
        return (earlier[0] + later[0], jnp.exp(later[0])[:, None] * earlier[1] + later[1])

    prefix = carried_in(
        (total_log, flat_state),
        "sp",
        combine,
        (jnp.zeros_like(total_log), jnp.zeros_like(flat_state)),
    )
    carried = prefix[1]
    entering_all = (
        entering + jnp.exp(lead_log)[:, :, None, None] * carried.reshape(final_state.shape)[None]
    )
    outer = jnp.einsum(
        "cihn,chpn->cihp", c_heads * jnp.exp(cum_log)[..., None], entering_all, precision=HIGH
    )
    core = (inner + outer).reshape(length, -1)
    gated = core * jax.nn.silu(z_stream.astype(jnp.float32))
    grouped = gated.reshape(length, groups, -1)
    grouped = grouped * lax.rsqrt(jnp.mean(grouped * grouped, axis=-1, keepdims=True) + EPS)
    ssd_out = grouped.reshape(length, -1) * group_gain
    gates = jax.nn.sigmoid(gate_pre)
    ssd_gate = jnp.repeat(gates[:, 0, :], HEAD_DIM, axis=1)
    short_gate = jnp.repeat(gates[:, 1, :], HEAD_DIM, axis=1)
    merged = (ssd_gate * ssd_out + short_gate * short_out).astype(jnp.bfloat16)
    partial_value = lax.dot_general(
        merged,
        gathered_by_axis(w_out, ("sp", "fs"), 0),
        (((1,), (1,)), ((), ())),
        preferred_element_type=jnp.float32,
    )
    mixed = sent_and_summed(partial_value.astype(jnp.bfloat16), "tp", 0).astype(jnp.bfloat16)
    return mixed[None]


def solution(mesh):
    return jax.shard_map(
        body,
        mesh=mesh,
        in_specs=(
            P(("grp", "fs"), "sp", "tp"),
            P(),
            P(("sp", "fs"), "tp"),
            P(("sp", "fs"), "tp"),
            P(("sp", "fs"), "tp"),
            P(("sp", "fs"), "tp"),
            P(None, "tp"),
            P(None, None, "tp"),
            P(("sp", "fs"), "tp"),
            P(("sp", "fs"), "tp"),
            P(("sp", "fs"), "tp"),
            P(None, "tp"),
            P(None, "tp"),
            P(None, "tp"),
            P(None, "tp"),
            P("tp"),
            P("tp"),
            P("tp"),
            P(("grp", "fs"), "sp"),
            P(("sp", "fs"), "tp"),
        ),
        out_specs=P(("grp", "fs"), ("sp", "tp"), None),
        check_vma=False,
    )
```

profile of v0, /device:TPU:33, one launch (start us, length us, event | category | flops | bytes accessed | tf_op | source)
XLA Modules:
  0.0 389.0 jit_solution(4231696968002133204)
XLA Ops:
  6.6 1.0 broadcast_in_dim.38
  7.6 24.2 %all_to_all.197 = bf16[2,128,1024]{2,1,0:T(8,128)(2,1)S(1)} all-to-all(bf16[2,128,1024]{2,1,0:T(8,128)(2,1)S(1)} %broadcast_in_dim.38), channel_id=1, replica_groups=mesh['grp'=2,'sp'=16,'fs'=4,'tp'=2] {'tp'}, dimensions={0} | all-to-all | bytes 1048576 | tf_op jit(solution)/shard_map/all_to_all | solution.py:23
  32.9 1.0 copy.125
  34.8 3.3 all-to-all-start.3
  39.0 3.3 all-to-all-done.3
  42.3 3.3 all-to-all-start.4
  46.3 3.6 all-to-all-done.4
  49.9 3.4 all-to-all-start.1
  53.9 4.6 %all-to-all-done.1 = bf16[32,4,256]{2,0,1:T(8,128)(2,1)S(1)} async-done(((bf16[32,4,256]{2,0,1:T(8,128)(2,1)}), bf16[32,4,256]{2,0,1:T(8,128)(2,1)S(1)}, u32[]{:S(2)}, u32[]{:S(2)}) %all-to-all-start.1) | async-done | bytes 65568 | tf_op jit(solution)/shard_map/all_to_all | solution.py:123
  58.5 3.4 all-to-all-start.2
  62.6 4.2 %all-to-all-done.2 = bf16[32,4,256]{2,0,1:T(8,128)(2,1)S(1)} async-done(((bf16[32,4,256]{2,0,1:T(8,128)(2,1)}), bf16[32,4,256]{2,0,1:T(8,128)(2,1)S(1)}, u32[]{:S(2)}, u32[]{:S(2)}) %all-to-all-start.2) | async-done | bytes 65568 | tf_op jit(solution)/shard_map/all_to_all | solution.py:124
  66.7 3.5 all-to-all-start.5
  70.9 3.7 all-to-all-done.5
  74.6 3.4 all-to-all-start.6
  78.7 3.7 all-to-all-done.6
  82.4 3.4 all-to-all-start.7
  86.0 4.1 %all-to-all-done.7 = bf16[32,4,256]{2,0,1:T(8,128)(2,1)S(1)} async-done(((bf16[32,4,256]{2,0,1:T(8,128)(2,1)}), bf16[32,4,256]{2,0,1:T(8,128)(2,1)S(1)}, u32[]{:S(2)}, u32[]{:S(2)}) %all-to-all-start.7) | async-done | bytes 65568 | tf_op jit(solution)/shard_map/all_to_all | solution.py:129
  95.8 73.5 %all-gather.8.cloned.1.call-done = bf16[2048,1408]{1,0:T(8,128)(2,1)} async-done(((bf16[128,1408]{1,0:T(8,128)(2,1)}), bf16[2048,1408]{1,0:T(8,128)(2,1)}) %all-gather.8.cloned.1.call-update) | async-done | bytes 5767184 | tf_op jit(solution)/shard_map/all_gather | solution.py:33
  169.3 3.4 convolution_convert_fusion.4
  172.7 1.1 copy.134
  173.8 2.6 convolution_convert_fusion.5
  176.5 1.8 copy.133
  178.3 2.0 fusion.6
  180.3 1.8 fusion.5
  182.8 4.0 %all-to-all-start.9 = ((bf16[4,256,64]{1,2,0:T(8,128)(2,1)}), bf16[4,256,64]{1,2,0:T(8,128)(2,1)S(1)}, u32[]{:S(2)}, u32[]{:S(2)}) async-start(bf16[4,256,64]{1,2,0:T(8,128)(2,1)} %pad_maximum_fusion.2), calls=%async_computation.9 | async-start | bytes 262144 | tf_op jit(solution)/shard_map/all_to_all | solution.py:40
  186.8 1.8 pad_maximum_fusion.1
  188.7 3.0 all-to-all-done.9
  191.7 3.6 all-to-all-start.8
  196.0 2.0 collective-permute-start.1
  200.2 1.9 all-to-all-done.8
  202.2 2.2 collective-permute-start
  205.3 2.9 collective-permute-done
  208.5 1.2 divide_multiply_fusion
  210.2 1.2 broadcast_multiply_fusion
  211.4 1.4 copy.146
  212.9 2.4 fusion.23
  215.4 2.0 while.27
  218.6 10.4 %all_gather.24 = bf16[128,1024]{1,0:T(8,128)(2,1)} all-gather(bf16[32,1024]{1,0:T(8,128)(2,1)S(1)} %copy-done.16), channel_id=1, replica_groups=mesh['grp'=2,'sp'=16,'fs'=4,'tp'=2] {'fs'}, dimensions={0}, use_global_device_ids=true | all-gather | bytes 327680 | tf_op jit(solution)/shard_map/all_gather | solution.py:71
  230.9 25.1 %all-reduce = bf16[256]{0:T(256)(128)(2,1)S(1)} all-reduce(bf16[256]{0:T(256)(128)(2,1)S(1)} %dynamic-update-slice), channel_id=2, replica_groups=mesh['grp'=2,'sp'=16,'fs'=4,'tp'=2] {'sp'}, use_global_device_ids=true, to_apply=%add | all-reduce | flops 256 | bytes 1024
  257.2 2.6 convolution_convert_fusion.1
  260.0 2.6 convolution_convert_fusion.2
  262.8 2.6 convolution_convert_fusion.3
  265.6 4.1 %collective-permute-start.2 = (bf16[3,256]{0,1:T(8,128)(2,1)S(1)}, bf16[3,256]{0,1:T(8,128)(2,1)S(1)}, u32[]{:S(2)}, u32[]{:S(2)}) collective-permute-start(bf16[3,256]{0,1:T(8,128)(2,1)S(1)} %copy-done.22), channel_id=1, source_target_pairs={{0,8},{8,16},{16,24},{24,32},{32,40},{40,48},{48,56},{56,64},{64,7... | collective-permute-start | bytes 4616 | tf_op jit(solution)/shard_map/ppermute | solution.py:47
  270.7 4.5 %all-to-all-start.10 = ((bf16[4,384,256]{1,2,0:T(8,128)(2,1)}), bf16[4,384,256]{1,2,0:T(8,128)(2,1)}, u32[]{:S(2)}, u32[]{:S(2)}) async-start(bf16[4,384,256]{1,2,0:T(8,128)(2,1)} %pad_maximum_fusion), calls=%async_computation.10 | async-start | bytes 1572864 | tf_op jit(solution)/shard_map/all_to_all | solution.py:40
  276.1 2.8 fusion.4
  278.9 1.6 reshape.303
  280.5 2.2 fusion.58
  283.3 1.2 slice_bitcast_fusion.1
  284.5 2.0 collective-permute-start.3
  286.5 2.7 collective-permute-start.4
  289.3 1.1 slice_bitcast_fusion
  290.9 3.6 collective-permute-done.4
  295.0 17.0 %while.28 = (s32[]{:T(128)}, f32[16,4096]{1,0:T(8,128)S(1)}, s32[]{:T(128)}, bf16[16,16]{1,0:T(8,128)(2,1)S(1)}, bf16[16,16,4096]{2,1,0:T(8,128)(2,1)}, /*index=5*/s32[]{:T(128)}, s32[]{:T(128)}) while((s32[]{:T(128)}, f32[16,4096]{1,0:T(8,128)S(1)}, s32[]{:T(128)}, bf16[16,16]{1,0:T(8,128)(2,1)S(1)}, ...), condition=%wide.region_7.8_spmd.clone, body=%wide.region_6.7_spmd.clone.sunk | while | flops 327700 | bytes 655633 | solution.py:66
  295.0 1.1 fusion.79
  296.2 1.0 fusion.79
  298.3 1.0 fusion.79
  299.4 1.0 fusion.79
  300.4 1.0 fusion.79
  301.5 1.0 fusion.79
  312.3 4.1 %multiply_reduce_fusion = (f32[2,64,16]{1,2,0:T(8,128)S(1)}, f32[2,64,16,64]{1,3,2,0:T(8,128)S(1)}) fusion(f32[2,64,16,64]{1,0,3,2:T(2,128)} %reshape.303, f32[2,16,64,64]{3,2,1,0:T(8,128)} %fusion.58, f32[2,64,16,64]{3,1,2,0:T(8,128)S(1)} %bitcast.253, f32[2,64,16]{1,2,0:T(8,128)S(1)} %copy.150, f32[2,16,64,64]{3,2,1,0:T(8,128)} %get-tuple-element.127, ...), kind=kOutput, calls=%fused_computation.40 | convolution fusion | flops 102103040 | bytes 2900096 | tf_op jit(solution)/shard_map/cihn,chpn->cihp/dot_general | solution.py:230
  317.9 2.1 fusion.29
  320.0 44.3 %all-gather.12.cloned.1.call-done = bf16[2048,1024]{1,0:T(8,128)(2,1)} async-done(((bf16[128,1024]{1,0:T(8,128)(2,1)}), bf16[2048,1024]{1,0:T(8,128)(2,1)}) %all-gather.12.cloned.1.call-update) | async-done | bytes 4194320 | tf_op jit(solution)/shard_map/all_gather | solution.py:71
  364.3 3.7 convolution_convert_fusion
  368.0 13.6 %all_to_all.198 = bf16[2,64,2048]{2,1,0:T(8,128)(2,1)S(1)} all-to-all(bf16[2,64,2048]{2,1,0:T(8,128)(2,1)S(1)} %bitcast.255), channel_id=1, replica_groups=mesh['grp'=2,'sp'=16,'fs'=4,'tp'=2] {'tp'}, dimensions={0} | all-to-all | bytes 1048576 | tf_op jit(solution)/shard_map/all_to_all | solution.py:82
  (218 shorter events, 39.4 us)
Async XLA Ops:
  6.5 250.5 %copy-start = (bf16[2048,2,16]{0,2,1:T(8,128)(2,1)S(1)}, bf16[2048,2,16]{0,2,1:T(8,128)(2,1)}, u32[]{:S(2)}) copy-start(bf16[2048,2,16]{0,2,1:T(8,128)(2,1)} %param.31) | copy-start | bytes 393220
  6.6 89.2 %all-gather.6.cloned.1.call-start = ((), (), s32[]{:S(2)}) async-start(), calls=%async_computation.12 | async-start | bytes 2621440 | tf_op jit(solution)/shard_map/all_gather | solution.py:131
  7.6 24.9 %copy-start.14 = (f32[2048]{0:T(1024)S(1)}, f32[2048]{0:T(1024)}, u32[]{:S(2)}) copy-start(f32[2048]{0:T(1024)} %param.25) | copy-start | bytes 24580
  32.4 1.6 copy-start.27
  32.4 5.8 %copy-start.28 = (bf16[32,256]{1,0:T(8,128)(2,1)S(1)}, bf16[32,256]{1,0:T(8,128)(2,1)}, u32[]{:S(2)}) copy-start(bf16[32,256]{1,0:T(8,128)(2,1)} %param.29) | copy-start | bytes 49156
  32.5 13.2 %copy-start.17 = (bf16[32,1024]{1,0:T(8,128)(2,1)S(1)}, bf16[32,1024]{1,0:T(8,128)(2,1)}, u32[]{:S(2)}) copy-start(bf16[32,1024]{1,0:T(8,128)(2,1)} %param.26) | copy-start | bytes 196612
  32.5 20.8 %copy-start.18 = (bf16[32,1024]{1,0:T(8,128)(2,1)S(1)}, bf16[32,1024]{1,0:T(8,128)(2,1)}, u32[]{:S(2)}) copy-start(bf16[32,1024]{1,0:T(8,128)(2,1)} %param.27) | copy-start | bytes 196612
  32.5 29.4 %copy-start.19 = (bf16[32,1024]{1,0:T(8,128)(2,1)S(1)}, bf16[32,1024]{1,0:T(8,128)(2,1)}, u32[]{:S(2)}) copy-start(bf16[32,1024]{1,0:T(8,128)(2,1)} %param.32) | copy-start | bytes 196612
  32.5 58.7 %copy-start.31 = (f32[128]{0:T(128)}, f32[128]{0:T(128)S(1)}, u32[]{:S(2)}) copy-start(f32[128]{0:T(128)S(1)} %add_rsqrt_fusion.1) | copy-start | bytes 1540
  32.5 37.7 %copy-start.20 = (bf16[32,1024]{1,0:T(8,128)(2,1)S(1)}, bf16[32,1024]{1,0:T(8,128)(2,1)}, u32[]{:S(2)}) copy-start(bf16[32,1024]{1,0:T(8,128)(2,1)} %param.33) | copy-start | bytes 196612
  32.6 45.5 %copy-start.21 = (bf16[32,1024]{1,0:T(8,128)(2,1)S(1)}, bf16[32,1024]{1,0:T(8,128)(2,1)}, u32[]{:S(2)}) copy-start(bf16[32,1024]{1,0:T(8,128)(2,1)} %param.34) | copy-start | bytes 196612
  32.9 58.2 %copy-start.41 = (f32[1,2]{1,0:T(1,128)S(1)}, f32[1,2]{1,0:T(1,128)}, u32[]{:S(2)}) copy-start(f32[1,2]{1,0:T(1,128)} %param.42) | copy-start | bytes 28
  34.0 57.6 %copy-start.15 = (bf16[2048,16]{0,1:T(8,128)(2,1)S(1)}, bf16[2048,16]{0,1:T(8,128)(2,1)}, u32[]{:S(2)}) copy-start(bf16[2048,16]{0,1:T(8,128)(2,1)} %param.30) | copy-start | bytes 196612
  34.0 57.6 %copy-start.39 = (f32[16]{0:T(128)S(1)}, f32[16]{0:T(128)}, u32[]{:S(2)}) copy-start(f32[16]{0:T(128)} %param.39) | copy-start | bytes 196
  34.8 7.5 %all-to-all-start.3 = ((bf16[4,2,1024]{2,1,0:T(2,128)(2,1)}), bf16[4,2,1024]{2,1,0:T(2,128)(2,1)S(1)}, u32[]{:S(2)}, u32[]{:S(2)}) async-start(bf16[4,2,1024]{2,1,0:T(2,128)(2,1)} %reshape.304), calls=%async_computation.3 | async-start | bytes 32768 | tf_op jit(solution)/shard_map/all_to_all | solution.py:125
  42.3 7.6 %all-to-all-start.4 = ((bf16[4,2,1024]{2,1,0:T(2,128)(2,1)}), bf16[4,2,1024]{2,1,0:T(2,128)(2,1)S(1)}, u32[]{:S(2)}, u32[]{:S(2)}) async-start(bf16[4,2,1024]{2,1,0:T(2,128)(2,1)} %reshape.306), calls=%async_computation.4 | async-start | bytes 32768 | tf_op jit(solution)/shard_map/all_to_all | solution.py:126
  46.3 45.6 %copy-start.42 = (f32[16]{0:T(128)S(1)}, f32[16]{0:T(128)}, u32[]{:S(2)}) copy-start(f32[16]{0:T(128)} %param.40) | copy-start | bytes 196
  49.9 8.6 %all-to-all-start.1 = ((bf16[32,4,256]{2,0,1:T(8,128)(2,1)}), bf16[32,4,256]{2,0,1:T(8,128)(2,1)S(1)}, u32[]{:S(2)}, u32[]{:S(2)}) async-start(bf16[32,4,256]{2,0,1:T(8,128)(2,1)} %bitcast.226), calls=%async_computation.1 | async-start | bytes 131072 | tf_op jit(solution)/shard_map/all_to_all | solution.py:123
  58.5 8.2 %all-to-all-start.2 = ((bf16[32,4,256]{2,0,1:T(8,128)(2,1)}), bf16[32,4,256]{2,0,1:T(8,128)(2,1)S(1)}, u32[]{:S(2)}, u32[]{:S(2)}) async-start(bf16[32,4,256]{2,0,1:T(8,128)(2,1)} %bitcast.225), calls=%async_computation.2 | async-start | bytes 131072 | tf_op jit(solution)/shard_map/all_to_all | solution.py:124
  66.7 27.8 %copy-start.37 = (f32[4,256]{1,0:T(4,128)S(1)}, f32[4,256]{1,0:T(4,128)}, u32[]{:S(2)}) copy-start(f32[4,256]{1,0:T(4,128)} %param.36) | copy-start | bytes 12292
  66.7 28.4 %copy-start.29 = (f32[4,1024]{1,0:T(4,128)S(1)}, f32[4,1024]{1,0:T(4,128)}, u32[]{:S(2)}) copy-start(f32[4,1024]{1,0:T(4,128)} %param.35) | copy-start | bytes 49156
  66.7 7.9 %all-to-all-start.5 = ((bf16[32,4,256]{2,0,1:T(8,128)(2,1)}), bf16[32,4,256]{2,0,1:T(8,128)(2,1)S(1)}, u32[]{:S(2)}, u32[]{:S(2)}) async-start(bf16[32,4,256]{2,0,1:T(8,128)(2,1)} %bitcast.224), calls=%async_computation.5 | async-start | bytes 131072 | tf_op jit(solution)/shard_map/all_to_all | solution.py:127
  74.6 7.8 %all-to-all-start.6 = ((bf16[32,4,256]{2,0,1:T(8,128)(2,1)}), bf16[32,4,256]{2,0,1:T(8,128)(2,1)S(1)}, u32[]{:S(2)}, u32[]{:S(2)}) async-start(bf16[32,4,256]{2,0,1:T(8,128)(2,1)} %bitcast.223), calls=%async_computation.6 | async-start | bytes 131072 | tf_op jit(solution)/shard_map/all_to_all | solution.py:128
  82.4 7.8 %all-to-all-start.7 = ((bf16[32,4,256]{2,0,1:T(8,128)(2,1)}), bf16[32,4,256]{2,0,1:T(8,128)(2,1)S(1)}, u32[]{:S(2)}, u32[]{:S(2)}) async-start(bf16[32,4,256]{2,0,1:T(8,128)(2,1)} %bitcast.222), calls=%async_computation.7 | async-start | bytes 131072 | tf_op jit(solution)/shard_map/all_to_all | solution.py:129
  85.8 83.5 %all-gather.8.cloned.1.call-start = ((), (), s32[]{:S(2)}) async-start(), calls=%async_computation.13 | async-start | bytes 6127616 | tf_op jit(solution)/shard_map/all_gather | solution.py:33
  91.9 0.6 copy-start.11
  92.7 76.6 %copy-start.9 = (f32[2,64,16]{2,1,0:T(8,128)}, f32[2,64,16]{2,1,0:T(8,128)S(1)}, u32[]{:S(2)}) copy-start(f32[2,64,16]{2,1,0:T(8,128)S(1)} %reduce_window_sum.22) | copy-start | bytes 24580
  93.2 76.1 %copy-start.25 = (f32[2,1,16]{2,1,0:T(1,128)}, f32[2,1,16]{2,1,0:T(1,128)S(1)}, u32[]{:S(2)}) copy-start(f32[2,1,16]{2,1,0:T(1,128)S(1)} %get-tuple-element.197) | copy-start | bytes 388
  169.3 4.5 %copy-start.2 = (bf16[4,128,2048]{2,1,0:T(8,128)(2,1)S(1)}, bf16[4,128,2048]{2,1,0:T(8,128)(2,1)}, u32[]{:S(2)}) copy-start(bf16[4,128,2048]{2,1,0:T(8,128)(2,1)} %all-gather.6.cloned.1.call-done) | copy-start | bytes 6291460
  182.1 17.4 %copy-start.33 = (f32[1,256]{1,0:T(1,128)S(1)}, f32[1,256]{1,0:T(1,128)}, u32[]{:S(2)}) copy-start(f32[1,256]{1,0:T(1,128)} %get-tuple-element.213) | copy-start | bytes 3076
  182.1 17.4 %copy-start.34 = (f32[1,256]{1,0:T(1,128)S(1)}, f32[1,256]{1,0:T(1,128)}, u32[]{:S(2)}) copy-start(f32[1,256]{1,0:T(1,128)} %get-tuple-element.214) | copy-start | bytes 3076
  182.1 17.4 %copy-start.35 = (f32[1,256]{1,0:T(1,128)S(1)}, f32[1,256]{1,0:T(1,128)}, u32[]{:S(2)}) copy-start(f32[1,256]{1,0:T(1,128)} %get-tuple-element.215) | copy-start | bytes 3076
  182.1 17.4 %copy-start.36 = (f32[1,256]{1,0:T(1,128)S(1)}, f32[1,256]{1,0:T(1,128)}, u32[]{:S(2)}) copy-start(f32[1,256]{1,0:T(1,128)} %get-tuple-element.216) | copy-start | bytes 3076
  182.8 8.8 %all-to-all-start.9 = ((bf16[4,256,64]{1,2,0:T(8,128)(2,1)}), bf16[4,256,64]{1,2,0:T(8,128)(2,1)S(1)}, u32[]{:S(2)}, u32[]{:S(2)}) async-start(bf16[4,256,64]{1,2,0:T(8,128)(2,1)} %pad_maximum_fusion.2), calls=%async_computation.9 | async-start | bytes 262144 | tf_op jit(solution)/shard_map/all_to_all | solution.py:40
  191.7 10.4 %all-to-all-start.8 = ((bf16[4,256,256]{1,2,0:T(8,128)(2,1)}), bf16[4,256,256]{1,2,0:T(8,128)(2,1)S(1)}, u32[]{:S(2)}, u32[]{:S(2)}) async-start(bf16[4,256,256]{1,2,0:T(8,128)(2,1)} %pad_maximum_fusion.1), calls=%async_computation.8 | async-start | bytes 1048576 | tf_op jit(solution)/shard_map/all_to_all | solution.py:40
  195.2 99.7 %all-gather.10.cloned.1.call-start = ((), (), s32[]{:S(2)}) async-start(), calls=%async_computation.14 | async-start | bytes 2228224 | tf_op jit(solution)/shard_map/all_gather | solution.py:53
  196.0 3.4 collective-permute-start.1
  199.9 8.7 %copy-start.23 = (f32[1,1024]{1,0:T(1,128)S(1)}, f32[1,1024]{1,0:T(1,128)}, u32[]{:S(2)}) copy-start(f32[1,1024]{1,0:T(1,128)} %get-tuple-element.207) | copy-start | bytes 12292
  199.9 8.7 %copy-start.24 = (f32[1,1024]{1,0:T(1,128)S(1)}, f32[1,1024]{1,0:T(1,128)}, u32[]{:S(2)}) copy-start(f32[1,1024]{1,0:T(1,128)} %get-tuple-element.208) | copy-start | bytes 12292
  202.1 7.6 %copy-start.3 = (bf16[4,256,256]{1,2,0:T(8,128)(2,1)}, bf16[4,256,256]{1,2,0:T(8,128)(2,1)S(1)}, u32[]{:S(2)}) copy-start(bf16[4,256,256]{1,2,0:T(8,128)(2,1)S(1)} %all-to-all-done.8) | copy-start | bytes 1572868
  202.2 6.1 %collective-permute-start = (bf16[3,1024]{0,1:T(8,128)(2,1)S(1)}, bf16[3,1024]{0,1:T(8,128)(2,1)S(1)}, u32[]{:S(2)}, u32[]{:S(2)}) collective-permute-start(bf16[3,1024]{0,1:T(8,128)(2,1)S(1)} %slice_bitcast_fusion.6), channel_id=1, source_target_pairs={{0,8},{8,16},{16,24},{24,32},{32,40},{40,48},{48,56},{56,64},{64,7... | collective-permute-start | bytes 18440 | tf_op jit(solution)/shard_map/ppermute | solution.py:47
  212.8 2.6 copy-start.26
  215.4 3.2 copy-start.16
  215.4 13.6 %copy-start.10 = (f32[2,64,16]{2,1,0:T(8,128)S(1)}, f32[2,64,16]{2,1,0:T(8,128)}, u32[]{:S(2)}) copy-start(f32[2,64,16]{2,1,0:T(8,128)} %copy-done.9) | copy-start | bytes 24580
  215.4 13.8 %copy-start.38 = (f32[4,256]{1,0:T(4,128)S(1)}, f32[4,256]{1,0:T(4,128)}, u32[]{:S(2)}) copy-start(f32[4,256]{1,0:T(4,128)} %param.37) | copy-start | bytes 12292
  215.4 13.8 %copy-start.12 = (f32[2,64,16]{2,1,0:T(8,128)S(1)}, f32[2,64,16]{2,1,0:T(8,128)}, u32[]{:S(2)}) copy-start(f32[2,64,16]{2,1,0:T(8,128)} %get-tuple-element.198) | copy-start | bytes 24580
  217.4 11.9 %copy-start.43 = (u32[256]{0:T(256)S(1)}, u32[256]{0:T(256)}, u32[]{:S(2)}) copy-start(u32[256]{0:T(256)} %constant.85) | copy-start | bytes 3076
  217.4 13.2 %copy-start.40 = (bf16[16]{0:T(256)(128)(2,1)S(1)}, bf16[16]{0:T(256)(128)(2,1)}, u32[]{:S(2)}) copy-start(bf16[16]{0:T(256)(128)(2,1)} %get-tuple-element.196) | copy-start | bytes 100
  217.4 38.6 %copy-start.30 = (f32[3,1024]{1,0:T(4,128)S(1)}, f32[3,1024]{1,0:T(4,128)}, u32[]{:S(2)}) copy-start(f32[3,1024]{1,0:T(4,128)} %param.38) | copy-start | bytes 36868
  217.4 39.2 %copy-start.32 = (f32[128]{0:T(128)S(1)}, f32[128]{0:T(128)}, u32[]{:S(2)}) copy-start(f32[128]{0:T(128)} %copy-done.31) | copy-start | bytes 1540
  218.5 145.8 %all-gather.12.cloned.1.call-start = ((), (), s32[]{:S(2)}) async-start(), calls=%async_computation.15 | async-start | bytes 4456448 | tf_op jit(solution)/shard_map/all_gather | solution.py:71
  262.8 2.8 copy-start.22
  265.4 9.8 %copy-start.13 = (bf16[128,256]{0,1:T(8,128)(2,1)S(1)}, bf16[128,256]{0,1:T(8,128)(2,1)}, u32[]{:S(2)}) copy-start(bf16[128,256]{0,1:T(8,128)(2,1)} %get-tuple-element.194) | copy-start | bytes 196612
  265.6 9.6 %collective-permute-start.2 = (bf16[3,256]{0,1:T(8,128)(2,1)S(1)}, bf16[3,256]{0,1:T(8,128)(2,1)S(1)}, u32[]{:S(2)}, u32[]{:S(2)}) collective-permute-start(bf16[3,256]{0,1:T(8,128)(2,1)S(1)} %copy-done.22), channel_id=1, source_target_pairs={{0,8},{8,16},{16,24},{24,32},{32,40},{40,48},{48,56},{56,64},{64,7... | collective-permute-start | bytes 4616 | tf_op jit(solution)/shard_map/ppermute | solution.py:47
  270.7 12.6 %all-to-all-start.10 = ((bf16[4,384,256]{1,2,0:T(8,128)(2,1)}), bf16[4,384,256]{1,2,0:T(8,128)(2,1)}, u32[]{:S(2)}, u32[]{:S(2)}) async-start(bf16[4,384,256]{1,2,0:T(8,128)(2,1)} %pad_maximum_fusion), calls=%async_computation.10 | async-start | bytes 1572864 | tf_op jit(solution)/shard_map/all_to_all | solution.py:40
  276.0 2.9 copy-start.8
  276.1 2.8 copy-start.6
  276.1 4.4 %copy-start.1 = (f32[2,64,16,64]{1,3,2,0:T(8,128)S(1)}, f32[2,64,16,64]{1,3,2,0:T(8,128)}, u32[]{:S(2)}) copy-start(f32[2,64,16,64]{1,3,2,0:T(8,128)} %copy.146) | copy-start | bytes 1572868
  278.9 1.6 copy-start.5
  284.5 6.4 %collective-permute-start.3 = (bf16[3,1024]{0,1:T(8,128)(2,1)S(1)}, bf16[3,1024]{0,1:T(8,128)(2,1)S(1)}, u32[]{:S(2)}, u32[]{:S(2)}) collective-permute-start(bf16[3,1024]{0,1:T(8,128)(2,1)S(1)} %get-tuple-element.187), channel_id=1, source_target_pairs={{0,8},{8,16},{16,24},{24,32},{32,40},{40,48},{48,56},{56,64},{64,7... | collective-permute-start | bytes 18440 | tf_op jit(solution)/shard_map/ppermute | solution.py:47
  286.5 8.0 %collective-permute-start.4 = (bf16[3,1024]{0,1:T(8,128)(2,1)S(1)}, bf16[3,1024]{0,1:T(8,128)(2,1)S(1)}, u32[]{:S(2)}, u32[]{:S(2)}) collective-permute-start(bf16[3,1024]{0,1:T(8,128)(2,1)S(1)} %get-tuple-element.186), channel_id=1, source_target_pairs={{0,8},{8,16},{16,24},{24,32},{32,40},{40,48},{48,56},{56,64},{64,7... | collective-permute-start | bytes 18440 | tf_op jit(solution)/shard_map/ppermute | solution.py:47
  295.0 17.3 %copy-start.7 = (f32[2,64,4,4,64]{4,1,3,2,0:T(8,128)S(1)}, f32[2,64,4,4,64]{4,1,3,2,0:T(8,128)}, u32[]{:S(2)}) copy-start(f32[2,64,4,4,64]{4,1,3,2,0:T(8,128)} %copy-done.6) | copy-start | bytes 1572868
  316.4 1.6 copy-start.4
Sparse Core Ops, SparseCore 0:
  34.1 32.0 all-gather.5
  91.2 78.0 all-gather.7
  218.6 69.9 all-gather.9
  290.2 74.0 all-gather.11
where the time goes:
time: 391 us; the launch traced here: 389 us
  waiting for transfers between devices  159 us (41%)
  blocking collectives  73.2 us (19%)
  starting transfers between devices  49 us (13%)
  matrix products  33.2 us (8%)
  other arithmetic  32.4 us (8%)
  local copies, waits for them, and re-layouts  27.1 us (7%)
  between operations  14.9 us (4%)
    all_gather x1, waiting for transfers between devices, in_one_piece(): filled = lax.all_gather(both, axis, axis=dim, tiled=True)  73.5 us
    all_gather x1, waiting for transfers between devices, gathered_by_axis(): x = lax.all_gather(x, axis, axis=dim, tiled=True)  44.3 us
    unnamed x1, blocking collectives  25.1 us
    all_to_all x1, blocking collectives, sent_to_all(): return lax.all_to_all(copies, axis, split_axis=0, concat_axis=0, tiled=True)  24.2 us
    dot_general x7, matrix products, body(): jnp.dot(stacked, weight, preferred_element_type=jnp.float32)  17.6 us
    select_n x16, other arithmetic, hop(): return jax.tree.map(lambda a, b: jnp.where(reached, a, b), new, before)  16.3 us
    all_to_all x1, blocking collectives, sent_and_summed(): lax.all_to_all(parts, axis, split_axis=0, concat_axis=0, tiled=True)  13.6 us
    ppermute x5, starting transfers between devices, from_behind(): return lax.ppermute(block, axis, route)  13.1 us
  transfers between devices with their start and end apart: 19, of which 16 were waited for; matrix products, arithmetic and copies ran while one was open for 16% of the time, Pallas kernels for 0%

commit v1 on v0

v1 whole, which is shorter than its diff:
```python
import functools

import jax
import jax.numpy as jnp
from jax import lax
from jax.experimental import pallas as pl
from jax.experimental.pallas import tpu as pltpu
from jax.sharding import PartitionSpec as P

HEAD_DIM = 64
STATE = 64
BLOCK = 64
EDGE = 8
EPS = 1.0
HIGH = lax.Precision.HIGHEST
F32 = jnp.float32
BF16 = jnp.bfloat16


def silu(v):
    return v / (1.0 + jnp.exp(-v))


def by_columns(w, size):
    rows, cols = w.shape
    return jnp.moveaxis(w.reshape(rows, size, cols // size), 1, 0)


def dot(a, b, contract=((1,), (0,))):
    return lax.dot_general(a, b, (contract, ((), ())), preferred_element_type=F32)


def scan_kernel(taps, heads, xbc_ref, taps_ref, step_ref, cum_ref, cumt_ref, inner_ref, c_ref, state_ref):
    length = inner_ref.shape[1]
    width = heads * HEAD_DIM
    stream = xbc_ref[0].astype(F32)
    conv = stream[EDGE - taps + 1 : EDGE - taps + 1 + length] * taps_ref[0:1]
    for k in range(1, taps):
        lo = EDGE - taps + 1 + k
        conv = conv + stream[lo : lo + length] * taps_ref[k : k + 1]
    conv = silu(conv)
    b = conv[:, width : width + STATE].astype(BF16)
    c = conv[:, width + STATE :].astype(BF16)
    c_ref[0] = c
    scores = dot(c, b, ((1,), (1,)))
    rows = lax.broadcasted_iota(jnp.int32, (length, length), 0)
    cols = lax.broadcasted_iota(jnp.int32, (length, length), 1)
    lower = rows >= cols
    for h in range(heads):
        cum = cum_ref[0, :, h : h + 1]
        gap = cum - cumt_ref[0, h : h + 1, :]
        decay = jnp.where(lower, jnp.exp(jnp.minimum(gap, 0.0)), 0.0)
        x_step = conv[:, h * HEAD_DIM : (h + 1) * HEAD_DIM] * step_ref[0, :, h : h + 1]
        inner_ref[0, :, h * HEAD_DIM : (h + 1) * HEAD_DIM] = dot((scores * decay).astype(BF16), x_step.astype(BF16))
        to_end = jnp.exp(cum[length - 1 : length] - cum)
        state_ref[0, h] = dot((x_step * to_end).astype(BF16), b, ((0,), (0,))).astype(BF16)


def merge_kernel(
    taps, heads, rest_ref, taps_ref, inner_ref, c_ref, cum_ref, prefix_ref, gate_ref, gain_ref, out_ref
):
    length = inner_ref.shape[1]
    width = heads * HEAD_DIM
    z = rest_ref[0, EDGE:, 0:width].astype(F32)
    scb = rest_ref[0, EDGE:, width : 2 * width].astype(F32)
    short_in = rest_ref[0, :, 2 * width : 3 * width].astype(F32) * rest_ref[0, :, 3 * width : 4 * width].astype(F32)
    first = EDGE - taps + 1
    conv = short_in[first : first + length] * taps_ref[0:1]
    for k in range(1, taps):
        conv = conv + short_in[first + k : first + k + length] * taps_ref[k : k + 1]
    short_out = scb * conv
    c = c_ref[0].astype(F32)
    outer = []
    for h in range(heads):
        scaled = (c * jnp.exp(cum_ref[0, :, h : h + 1])).astype(BF16)
        outer.append(dot(scaled, prefix_ref[0, h], ((1,), (1,))))
    core = inner_ref[0] + jnp.concatenate(outer, axis=1)
    gated = core * silu(z)
    scale = lax.rsqrt(jnp.mean(gated * gated, axis=1, keepdims=True) + EPS)
    ssd_out = gated * scale * gain_ref[...]
    gates = jax.nn.sigmoid(gate_ref[0])
    spread = lambda lo: jnp.concatenate(
        [jnp.broadcast_to(gates[:, lo + h : lo + h + 1], (length, HEAD_DIM)) for h in range(heads)], axis=1
    )
    out_ref[0] = (spread(0) * ssd_out + spread(heads) * short_out).astype(out_ref.dtype)


def whole(shape):
    return pl.BlockSpec(shape, lambda s: (0,) * len(shape))


def one(shape):
    return pl.BlockSpec((1, *shape), lambda s: (s,) + (0,) * len(shape))


def body(
    tokens,
    norm_gain,
    w_z,
    w_x,
    w_b,
    w_c,
    w_dt,
    w_gate,
    w_scb,
    w_scc,
    w_scx,
    conv_x,
    conv_b,
    conv_c,
    conv_sc,
    dt_bias,
    decay_log,
    group_gain,
    span_shift,
    w_out,
):
    sp, fs, tp = (lax.axis_size(a) for a in ("sp", "fs", "tp"))
    here_sp, here_fs = lax.axis_index("sp"), lax.axis_index("fs")
    own = tokens[0]
    length, half = own.shape
    heads = dt_bias.shape[0] // fs
    width = heads * HEAD_DIM

    def mine(a, dim):
        size = a.shape[dim] // fs
        return lax.dynamic_slice_in_dim(a, here_fs * size, size, dim)

    def exchanged(weights):
        packed = jnp.concatenate([by_columns(w, fs) for w in weights], axis=2)
        got = lax.all_to_all(packed, "fs", split_axis=0, concat_axis=0, tiled=True)
        return got.reshape(-1, got.shape[2])

    first = exchanged((w_x, w_b, w_c))
    rest = exchanged((w_z, w_scb, w_scc, w_scx, w_out))

    before = lax.ppermute(own[length - EDGE :], "sp", [(i, i + 1) for i in range(sp - 1)])
    block = jnp.concatenate([before, own], axis=0)
    shift = jnp.repeat(span_shift[0], BLOCK)
    block = lax.all_to_all(jnp.broadcast_to(block, (fs, *block.shape)), "fs", 0, 0, tiled=True)
    block = lax.all_to_all(jnp.broadcast_to(block, (tp, *block.shape)), "tp", 0, 0, tiled=True)
    shifts = lax.all_gather(shift, "fs")

    full_first = lax.all_gather(first, "sp", axis=0, tiled=True)
    full_rest = lax.all_gather(rest, "sp", axis=0, tiled=True)

    rows = jnp.concatenate([block[k] for k in range(tp)], axis=2).astype(F32)
    inverse_rms = lax.rsqrt(jnp.mean(rows * rows, axis=2, keepdims=True) + EPS)
    normed = (rows * inverse_rms * norm_gain).astype(BF16).reshape(-1, tp * half)

    narrow = jnp.concatenate([mine(w_dt, 1)] + [mine(w_gate[:, k], 1) for k in range(2)], axis=1)
    small = dot(normed, narrow).reshape(fs, EDGE + length, -1)[:, EDGE:]
    gate_pre = small[:, :, heads:]
    step = jax.nn.softplus(small[:, :, :heads] + mine(dt_bias, 0) + shifts[:, :, None])
    rate = -jnp.exp(mine(decay_log, 0))
    log_step = step * rate
    tri = (lax.iota(jnp.int32, length)[:, None] >= lax.iota(jnp.int32, length)[None, :]).astype(F32)
    cum = jnp.einsum("ij,sjh->sih", tri, log_step, precision=HIGH)
    cum_t = jnp.einsum("ij,sjh->shi", tri, log_step, precision=HIGH)
    total_log = cum_t[:, :, length - 1].reshape(-1)

    xbc = dot(normed, full_first).astype(BF16).reshape(fs, EDGE + length, -1)
    taps_xbc = jnp.concatenate([mine(conv_x, 1), mine(conv_b, 1), mine(conv_c, 1)], axis=1)
    taps = taps_xbc.shape[0]
    inner, c_conv, state = pl.pallas_call(
        functools.partial(scan_kernel, taps, heads),
        grid=(fs,),
        in_specs=[
            one(xbc.shape[1:]),
            whole(taps_xbc.shape),
            one(step.shape[1:]),
            one(cum.shape[1:]),
            one(cum_t.shape[1:]),
        ],
        out_specs=[one((length, width)), one((length, STATE)), one((heads, HEAD_DIM, STATE))],
        out_shape=[
            jax.ShapeDtypeStruct((fs, length, width), F32),
            jax.ShapeDtypeStruct((fs, length, STATE), BF16),
            jax.ShapeDtypeStruct((fs, heads, HEAD_DIM, STATE), BF16),
        ],
    )(xbc, taps_xbc, step, cum, cum_t)

    pairs = fs * heads
    per = pairs // sp
    lanes = 2 * STATE
    flat = state.reshape(pairs, -1, lanes)
    coarse = total_log.astype(BF16)
    left = total_log - coarse.astype(F32)
    middle = left.astype(BF16)
    fine = (left - middle.astype(F32)).astype(BF16)
    logs = jnp.stack([coarse, middle, fine], axis=1)
    logs = jnp.pad(logs, ((0, 0), (0, lanes - 3)))[:, None]
    packed = jnp.concatenate([flat, jnp.pad(logs, ((0, 0), (0, 7), (0, 0)))], axis=1)
    arrived = lax.all_to_all(packed, "sp", 0, 0, tiled=True)
    depth = flat.shape[1]
    logs_all = arrived[:, depth, :3].astype(F32).sum(axis=1).reshape(sp, per)
    source = lax.iota(jnp.int32, sp)
    upto = jnp.einsum("ij,jk->ik", (source[:, None] > source[None, :]).astype(F32), logs_all, precision=HIGH)
    gap = upto[:, None] - (upto + logs_all)[None]
    weight = jnp.where((source[:, None] > source[None, :])[:, :, None], jnp.exp(jnp.minimum(gap, 0.0)), 0.0)
    states_all = arrived[:, :depth].reshape(sp, per, -1).astype(F32)
    prefix = jnp.einsum("zkp,kpe->zpe", weight, states_all, precision=HIGH).astype(BF16)
    prefix = lax.all_to_all(prefix.reshape(sp * per, depth, lanes), "sp", 0, 0, tiled=True)
    prefix = prefix.reshape(fs, heads, HEAD_DIM, STATE)

    full_w = full_rest[:, : 4 * width]
    others = dot(normed, full_w).astype(BF16).reshape(fs, EDGE + length, -1)
    taps_sc = mine(conv_sc, 1)
    gain = mine(group_gain, 0)[None]
    merged = pl.pallas_call(
        functools.partial(merge_kernel, taps_sc.shape[0], heads),
        grid=(fs,),
        in_specs=[
            one(others.shape[1:]),
            whole(taps_sc.shape),
            one(inner.shape[1:]),
            one(c_conv.shape[1:]),
            one(cum.shape[1:]),
            one(prefix.shape[1:]),
            one(gate_pre.shape[1:]),
            whole(gain.shape),
        ],
        out_specs=one((length, width)),
        out_shape=jax.ShapeDtypeStruct((fs, length, width), BF16),
    )(others, taps_sc, inner, c_conv, cum, prefix, gate_pre, gain)

    partial = dot(merged.reshape(-1, width), full_rest[:, 4 * width :], ((1,), (1,))).astype(BF16)
    features = partial.shape[1]
    parts = partial.reshape(fs, tp, length // tp, features)
    parts = jnp.moveaxis(parts, 1, 0)
    parts = lax.all_to_all(parts, "tp", 0, 0, tiled=True).astype(F32).sum(axis=0).astype(BF16)
    mixed = lax.all_to_all(parts, "fs", 0, 0, tiled=True).astype(F32).sum(axis=0).astype(BF16)
    return mixed[None]


def solution(mesh):
    return jax.shard_map(
        body,
        mesh=mesh,
        in_specs=(
            P(("grp", "fs"), "sp", "tp"),
            P(),
            P(("sp", "fs"), "tp"),
            P(("sp", "fs"), "tp"),
            P(("sp", "fs"), "tp"),
            P(("sp", "fs"), "tp"),
            P(None, "tp"),
            P(None, None, "tp"),
            P(("sp", "fs"), "tp"),
            P(("sp", "fs"), "tp"),
            P(("sp", "fs"), "tp"),
            P(None, "tp"),
            P(None, "tp"),
            P(None, "tp"),
            P(None, "tp"),
            P("tp"),
            P("tp"),
            P("tp"),
            P(("grp", "fs"), "sp"),
            P(("sp", "fs"), "tp"),
        ),
        out_specs=P(("grp", "fs"), ("sp", "tp"), None),
        check_vma=False,
    )
```

time: 391 us -> 235 us (0.60)
  waiting for transfers between devices: 159 us -> 54.8 us
  starting transfers between devices: 49 us -> 12.7 us
  blocking collectives: 73.2 us -> 106 us
  other arithmetic: 32.4 us -> 3.39 us
  matrix products: 33.2 us -> 13.3 us
  Pallas kernels: 0 us -> 9.63 us
  local copies, waits for them, and re-layouts: 27.1 us -> 19.6 us
    all_gather x4 -> x2, waiting for transfers between devices: 118 us -> 44.9 us  [the longest x1 40.3 us: body(): full_rest = lax.all_gather(rest, 'sp', axis=0, tiled=True)]
    all_to_all x2 -> x6, blocking collectives: 37.8 us -> 93.3 us  [the longest x1 25 us: body(): lax.all_to_all(jnp.broadcast_to(block, (tp, *block.shape)), 'tp', 0, 0, t...]
    all_to_all x10 -> x2, starting transfers between devices: 35.8 us -> 8.03 us  [the longest x1 4.41 us: body(): lax.all_to_all(prefix.reshape(sp * per, depth, lanes), 'sp', 0, 0, tiled=...]
    unnamed x1 -> x0, blocking collectives: 25.1 us -> none
    all_to_all x10 -> x2, waiting for transfers between devices: 32.7 us -> 9.79 us  [the longest x1 9.79 us: body(): lax.all_to_all(prefix.reshape(sp * per, depth, lanes), 'sp', 0, 0, tiled=...]
    dot_general x14 -> x7, matrix products: 33.2 us -> 13.3 us  [the longest x4 12.5 us: dot(): lax.dot_general(a, b, (contract, ((), ())), preferred_element_type=F32)]
    select_n x16 -> x1, other arithmetic: 16.3 us -> 0.22 us  [body(): jax.nn.softplus(small[:, :, :heads] + mine(dt_bias, 0) + shifts[:, :, None])]
    pallas_call x0 -> x2, Pallas kernels: none -> 9.63 us  [the longest x1 5.35 us: body(): pl.pallas_call(functools.partial(scan_kernel, taps, heads), grid=(fs,), i...]
  transfers between devices with their start and end apart: 19 -> 5, of which waited for: 16 -> 3; matrix products, arithmetic and copies ran while one was open for 16% -> 10% of each run, Pallas kernels for 0% -> 2%
where the time goes in v1:
time: 235 us; the launch traced here: 234 us
  blocking collectives  106 us (45%)
  waiting for transfers between devices  54.8 us (23%)
  local copies, waits for them, and re-layouts  19.6 us (8%)
  between operations  13.8 us (6%)
  matrix products  13.3 us (6%)
  starting transfers between devices  12.7 us (5%)
  Pallas kernels  9.63 us (4%)
  other arithmetic  3.39 us (1%)
    all_gather x1, waiting for transfers between devices, body(): full_rest = lax.all_gather(rest, 'sp', axis=0, tiled=True)  40.3 us
    all_to_all x1, blocking collectives, body(): lax.all_to_all(jnp.broadcast_to(block, (tp, *block.shape)), 'tp', 0, 0, t...  25 us
    all_to_all x1, blocking collectives, body(): arrived = lax.all_to_all(packed, 'sp', 0, 0, tiled=True)  18.8 us
    all_to_all x2, blocking collectives, exchanged(): got = lax.all_to_all(packed, 'fs', split_axis=0, concat_axis=0, tiled=True)  18.7 us
    all_to_all x1, blocking collectives, body(): lax.all_to_all(parts, 'fs', 0, 0, tiled=True).astype(F32).sum(axis=0)  17.9 us
    all_gather x1, blocking collectives, body(): shifts = lax.all_gather(shift, 'fs')  13.1 us
    all_to_all x1, blocking collectives, body(): lax.all_to_all(parts, 'tp', 0, 0, tiled=True).astype(F32).sum(axis=0)  12.9 us
    dot_general x4, matrix products, dot(): lax.dot_general(a, b, (contract, ((), ())), preferred_element_type=F32)  12.5 us
  transfers between devices with their start and end apart: 5, of which 3 were waited for; matrix products, arithmetic and copies ran while one was open for 10% of the time, Pallas kernels for 2%

profile of v1, /device:TPU:33, one launch (start us, length us, event | category | flops | bytes accessed | tf_op | source)
XLA Modules:
  0.0 233.6 jit_solution(4419026464849497296)
XLA Ops:
  6.6 0.1 all-gather.6.cloned.1.call-start
  6.6 0.9 reshape.201
  7.5 0.8 reshape.202
  8.3 0.8 reshape.203
  9.2 0.1 pad_maximum_fusion.3
  9.3 9.7 %all_to_all.40 = bf16[4,32,384]{2,1,0:T(8,128)(2,1)} all-to-all(bf16[4,32,384]{2,1,0:T(8,128)(2,1)S(1)} %copy.55), channel_id=1, replica_groups=mesh['grp'=2,'sp'=16,'fs'=4,'tp'=2] {'fs'}, dimensions={0} | all-to-all | bytes 196608 | tf_op jit(solution)/shard_map/all_to_all | solution.py:131
  19.0 0.1 all-gather.6.cloned.1.call-update
  19.0 0.1 all-gather.4.cloned.1.call-start
  19.1 0.9 reshape.194
  20.0 0.9 reshape.195
  20.8 0.9 reshape.196
  21.7 0.9 reshape.197
  22.6 0.9 reshape.198
  23.7 9.0 %all_to_all.41 = bf16[4,32,1280]{2,1,0:T(8,128)(2,1)} all-to-all(bf16[4,32,1280]{2,1,0:T(8,128)(2,1)S(1)} %copy.54), channel_id=1, replica_groups=mesh['grp'=2,'sp'=16,'fs'=4,'tp'=2] {'fs'}, dimensions={0} | all-to-all | bytes 655360 | tf_op jit(solution)/shard_map/all_to_all | solution.py:131
  32.7 0.1 all-gather.4.cloned.1.call-update
  32.9 4.6 %collective-permute-start = (bf16[8,1024]{1,0:T(8,128)(2,1)S(1)}, bf16[8,1024]{1,0:T(8,128)(2,1)S(1)}, u32[]{:S(2)}, u32[]{:S(2)}) collective-permute-start(bf16[8,1024]{1,0:T(8,128)(2,1)S(1)} %slice_bitcast_fusion), channel_id=1, source_target_pairs={{0,8},{8,16},{16,24},{24,32},{32,40},{40,48},{48,56},{56,64},{64,7... | collective-permute-start | bytes 49160 | tf_op jit(solution)/shard_map/ppermute | solution.py:137
  37.4 0.7 constant_dynamic-slice_fusion.3
  38.2 0.1 constant_dynamic-slice_fusion.1
  38.3 1.1 broadcast_in_dim.13
  39.4 3.6 %all-to-all-start = ((bf16[4,136,1024]{2,1,0:T(8,128)(2,1)}), bf16[4,136,1024]{2,1,0:T(8,128)(2,1)S(1)}, u32[]{:S(2)}, u32[]{:S(2)}) async-start(bf16[4,136,1024]{2,1,0:T(8,128)(2,1)} %broadcast_in_dim.13), calls=%async_computation | async-start | bytes 2228224 | tf_op jit(solution)/shard_map/all_to_all | solution.py:140
  43.1 0.1 exponential_negate_fusion
  43.1 0.1 dynamic_slice.43
  43.2 0.1 broadcast_in_dim.15
  43.3 0.1 reshape.212
  43.4 13.1 %all-gather = f32[4,1,128]{2,1,0:T(1,128)S(1)} all-gather(f32[1,1,128]{2,1,0:T(1,128)S(1)} %reshape.212), channel_id=1, replica_groups=mesh['grp'=2,'sp'=16,'fs'=4,'tp'=2] {'fs'}, dimensions={0}, use_global_device_ids=true | all-gather | bytes 2560 | tf_op jit(solution)/shard_map/all_gather | solution.py:142
  56.4 0.7 pad_maximum_fusion.4.taps_ref
  57.2 0.3 broadcast_in_dim.14
  57.5 25.0 %all_to_all.42 = bf16[2,4,136,1024]{3,2,1,0:T(8,128)(2,1)S(1)} all-to-all(bf16[2,4,136,1024]{3,2,1,0:T(8,128)(2,1)S(1)} %broadcast_in_dim.14), channel_id=1, replica_groups=mesh['grp'=2,'sp'=16,'fs'=4,'tp'=2] {'tp'}, dimensions={0} | all-to-all | bytes 4456448 | tf_op jit(solution)/shard_map/all_to_all | solution.py:141
  82.5 1.6 slice_bitcast_fusion.2
  84.1 0.5 fusion
  84.6 0.1 rsqrt.13
  84.7 0.1 copy-done.10
  84.8 0.8 fusion.5
  85.6 0.7 copy-done.3
  86.3 0.2 compare_select_fusion.step_ref
  86.5 0.3 fusion.16.cumt_ref
  86.9 0.9 copy.60
  87.8 0.2 slice_reduce_fusion
  87.9 0.1 reshape_squeeze.3
  88.0 0.1 copy.66
  88.1 4.6 %all-gather.6.cloned.1.call-done = bf16[2048,384]{1,0:T(8,128)(2,1)} async-done(((bf16[128,384]{1,0:T(8,128)(2,1)}), bf16[2048,384]{1,0:T(8,128)(2,1)}) %all-gather.6.cloned.1.call-update) | async-done | bytes 1572880 | tf_op jit(solution)/shard_map/all_gather | solution.py:144
  92.7 3.9 %convolution_convert_fusion.2 = bf16[544,384]{1,0:T(8,128)(2,1)} fusion(bf16[2048,384]{1,0:T(8,128)(2,1)} %all-gather.6.cloned.1.call-done, bf16[544,1024]{1,0:T(8,128)(2,1)S(1)} %bitcast.76, bf16[544,1024]{1,0:T(8,128)(2,1)} %bitcast.78, f32[2048]{0:T(1024)S(1)} %copy-done.10, f32[544]{0:T(1024)S(1)} %rsqrt.13), kind=kOutput, calls=%fused_computation.16 | convolution fusion | flops 863645696 | bytes 4229248 | tf_op jit(solution)/shard_map/dot_general | solution.py:30
  96.6 5.3 %shard_map.190 = (f32[4,128,256]{2,1,0:T(8,128)}, bf16[4,128,64]{2,1,0:T(8,128)(2,1)}, bf16[4,4,64,64]{3,2,1,0:T(8,128)(2,1)}) custom-call(bf16[4,136,384]{2,1,0:T(8,128)(2,1)} %bitcast.83, f32[4,384]{1,0:T(4,128)} %pad_maximum_fusion.4.taps_ref, f32[4,128,4]{2,1,0:T(8,128)} %copy-done.1, f32[4,128,4]{2,1,0:T(8,128)} %bitcast.73, f32[4,4,128]{2,1,0:T(4,128)} %copy-done.6), custom_call_target="tpu_custom_call" | custom-call | tf_op jit(solution)/shard_map/pallas_call | solution.py:165
  102.0 1.1 reshape.206
  103.1 18.8 %all_to_all.43 = bf16[16,40,128]{2,1,0:T(8,128)(2,1)S(1)} all-to-all(bf16[16,40,128]{2,1,0:T(8,128)(2,1)S(1)} %fusion.18), channel_id=1, replica_groups=mesh['grp'=2,'sp'=16,'fs'=4,'tp'=2] {'sp'}, dimensions={0} | all-to-all | bytes 327680 | tf_op jit(solution)/shard_map/all_to_all | solution.py:194
  122.0 0.2 fusion.34
  122.2 0.1 fusion.48
  122.3 0.3 fusion.12
  122.6 0.7 copy.68
  123.3 4.4 %all-to-all-start.5 = ((bf16[16,32,128]{2,1,0:T(8,128)(2,1)}), bf16[16,32,128]{2,1,0:T(8,128)(2,1)S(1)}, u32[]{:S(2)}, u32[]{:S(2)}) async-start(bf16[16,32,128]{2,1,0:T(8,128)(2,1)} %bitcast.42), calls=%async_computation.5 | async-start | bytes 262144 | tf_op jit(solution)/shard_map/all_to_all | solution.py:203
  127.7 1.3 dynamic_slice.45
  129.0 1.3 constant_dynamic-slice_fusion.4.taps_ref
  130.3 0.8 slice.62.gate_ref
  131.1 9.8 %all-to-all-done.5 = bf16[16,32,128]{2,1,0:T(8,128)(2,1)S(1)} async-done(((bf16[16,32,128]{2,1,0:T(8,128)(2,1)}), bf16[16,32,128]{2,1,0:T(8,128)(2,1)S(1)}, u32[]{:S(2)}, u32[]{:S(2)}) %all-to-all-start.5) | async-done | bytes 131104 | tf_op jit(solution)/shard_map/all_to_all | solution.py:203
  140.9 0.8 reshape.209.prefix_ref
  141.8 40.3 %all-gather.4.cloned.1.call-done = bf16[2048,1280]{1,0:T(8,128)(2,1)} async-done(((bf16[128,1280]{1,0:T(8,128)(2,1)}), bf16[2048,1280]{1,0:T(8,128)(2,1)}) %all-gather.4.cloned.1.call-update) | async-done | bytes 5242896 | tf_op jit(solution)/shard_map/all_gather | solution.py:145
  182.1 5.7 %fusion.9 = bf16[544,1024]{1,0:T(8,128)(2,1)} fusion(bf16[2048,1280]{1,0:T(8,128)(2,1)} %all-gather.4.cloned.1.call-done, bf16[544,1024]{1,0:T(8,128)(2,1)S(1)} %bitcast.77, bf16[544,1024]{1,0:T(8,128)(2,1)S(1)} %bitcast.79, f32[2048]{0:T(1024)S(1)} %copy-done.10, f32[544]{0:T(1024)S(1)} %rsqrt.13), kind=kOutput, calls=%fused_computation.15 | convolution fusion | flops 2290057216 | bytes 7547008 | tf_op jit(solution)/shard_map/dot_general | solution.py:30
  187.8 4.3 %shard_map.191 = bf16[4,128,256]{2,1,0:T(8,128)(2,1)} custom-call(bf16[4,136,1024]{2,1,0:T(8,128)(2,1)} %bitcast.80, f32[3,256]{1,0:T(4,128)} %constant_dynamic-slice_fusion.4.taps_ref, f32[4,128,256]{2,1,0:T(8,128)} %get-tuple-element.8.inner_ref, bf16[4,128,64]{2,1,0:T(8,128)(2,1)} %get-tuple-element.9.c_ref, f32[4,128,4]{2,1,0:T(8,128)} %bitcast.74, ...), custom_call_target="tpu_custom_call" | custom-call | tf_op jit(solution)/shard_map/pallas_call | solution.py:210
  192.1 2.0 convolution_convert_fusion.1
  194.2 0.2 copy.74
  194.4 12.9 %all_to_all.44 = bf16[2,4,64,2048]{3,2,1,0:T(8,128)(2,1)S(1)} all-to-all(bf16[2,4,64,2048]{3,2,1,0:T(8,128)(2,1)S(1)} %bitcast.72), channel_id=1, replica_groups=mesh['grp'=2,'sp'=16,'fs'=4,'tp'=2] {'tp'}, dimensions={0} | all-to-all | bytes 4194304 | tf_op jit(solution)/shard_map/all_to_all | solution.py:231
  207.3 0.6 reduce_sum.44
  207.9 17.9 %all_to_all.45 = bf16[4,64,2048]{2,1,0:T(8,128)(2,1)S(1)} all-to-all(bf16[4,64,2048]{2,1,0:T(8,128)(2,1)S(1)} %reduce_sum.44), channel_id=1, replica_groups=mesh['grp'=2,'sp'=16,'fs'=4,'tp'=2] {'fs'}, dimensions={0} | all-to-all | bytes 2097152 | tf_op jit(solution)/shard_map/all_to_all | solution.py:232
  225.9 0.9 reduce_sum.45
  (45 shorter events, 0.4 us)
Async XLA Ops:
  6.5 31.6 %copy-start = (bf16[2048,16]{0,1:T(8,128)(2,1)S(1)}, bf16[2048,16]{0,1:T(8,128)(2,1)}, u32[]{:S(2)}) copy-start(bf16[2048,16]{0,1:T(8,128)(2,1)} %param.26) | copy-start | bytes 196612
  6.6 26.2 %copy-start.5 = (bf16[1,128,1024]{2,1,0:T(8,128)(2,1)S(1)}, bf16[1,128,1024]{2,1,0:T(8,128)(2,1)}, u32[]{:S(2)}) copy-start(bf16[1,128,1024]{2,1,0:T(8,128)(2,1)} %param.20) | copy-start | bytes 786436
  6.6 31.6 %copy-start.9 = (f32[4,256]{1,0:T(4,128)S(1)}, f32[4,256]{1,0:T(4,128)}, u32[]{:S(2)}) copy-start(f32[4,256]{1,0:T(4,128)} %param.32) | copy-start | bytes 12292
  6.6 31.6 %copy-start.8 = (f32[4,256]{1,0:T(4,128)S(1)}, f32[4,256]{1,0:T(4,128)}, u32[]{:S(2)}) copy-start(f32[4,256]{1,0:T(4,128)} %param.33) | copy-start | bytes 12292
  6.6 86.1 %all-gather.6.cloned.1.call-start = ((), (), s32[]{:S(2)}) async-start(), calls=%async_computation.9 | async-start | bytes 1671168 | tf_op jit(solution)/shard_map/all_gather | solution.py:144
  19.0 163.1 %all-gather.4.cloned.1.call-start = ((), (), s32[]{:S(2)}) async-start(), calls=%async_computation.8 | async-start | bytes 5570560 | tf_op jit(solution)/shard_map/all_gather | solution.py:145
  32.8 10.3 %copy-start.11 = (f32[16]{0:T(128)S(1)}, f32[16]{0:T(128)}, u32[]{:S(2)}) copy-start(f32[16]{0:T(128)} %param.36) | copy-start | bytes 196
  32.8 10.3 %copy-start.12 = (f32[16]{0:T(128)S(1)}, f32[16]{0:T(128)}, u32[]{:S(2)}) copy-start(f32[16]{0:T(128)} %param.35) | copy-start | bytes 196
  32.8 10.4 %copy-start.13 = (f32[1,2]{1,0:T(1,128)S(1)}, f32[1,2]{1,0:T(1,128)}, u32[]{:S(2)}) copy-start(f32[1,2]{1,0:T(1,128)} %param.38) | copy-start | bytes 28
  32.8 24.3 %copy-start.7 = (bf16[2048,2,16]{0,2,1:T(8,128)(2,1)S(1)}, bf16[2048,2,16]{0,2,1:T(8,128)(2,1)}, u32[]{:S(2)}) copy-start(bf16[2048,2,16]{0,2,1:T(8,128)(2,1)} %param.27) | copy-start | bytes 393220
  32.9 5.4 %collective-permute-start = (bf16[8,1024]{1,0:T(8,128)(2,1)S(1)}, bf16[8,1024]{1,0:T(8,128)(2,1)S(1)}, u32[]{:S(2)}, u32[]{:S(2)}) collective-permute-start(bf16[8,1024]{1,0:T(8,128)(2,1)S(1)} %slice_bitcast_fusion), channel_id=1, source_target_pairs={{0,8},{8,16},{16,24},{24,32},{32,40},{40,48},{48,56},{56,64},{64,7... | collective-permute-start | bytes 49160 | tf_op jit(solution)/shard_map/ppermute | solution.py:137
  39.4 17.7 %all-to-all-start = ((bf16[4,136,1024]{2,1,0:T(8,128)(2,1)}), bf16[4,136,1024]{2,1,0:T(8,128)(2,1)S(1)}, u32[]{:S(2)}, u32[]{:S(2)}) async-start(bf16[4,136,1024]{2,1,0:T(8,128)(2,1)} %broadcast_in_dim.13), calls=%async_computation | async-start | bytes 2228224 | tf_op jit(solution)/shard_map/all_to_all | solution.py:140
  84.1 0.7 copy-start.10
  85.6 0.7 copy-start.3
  86.5 10.1 %copy-start.1 = (f32[4,128,4]{2,1,0:T(8,128)}, f32[4,128,4]{2,1,0:T(8,128)S(1)}, u32[]{:S(2)}) copy-start(f32[4,128,4]{2,1,0:T(8,128)S(1)} %compare_select_fusion.step_ref) | copy-start | bytes 24580
  86.9 9.7 %copy-start.6 = (f32[4,4,128]{2,1,0:T(4,128)}, f32[4,4,128]{2,1,0:T(4,128)S(1)}, u32[]{:S(2)}) copy-start(f32[4,4,128]{2,1,0:T(4,128)S(1)} %fusion.16.cumt_ref) | copy-start | bytes 24580
  96.6 33.7 %copy-start.4 = (f32[4,136,12]{2,1,0:T(8,128)S(1)}, f32[4,136,12]{2,1,0:T(8,128)}, u32[]{:S(2)}) copy-start(f32[4,136,12]{2,1,0:T(8,128)} %copy-done.3) | copy-start | bytes 78340
  96.6 85.5 %copy-start.2 = (bf16[1,4,136,1024]{3,2,1,0:T(8,128)(2,1)S(1)}, bf16[1,4,136,1024]{3,2,1,0:T(8,128)(2,1)}, u32[]{:S(2)}) copy-start(bf16[1,4,136,1024]{3,2,1,0:T(8,128)(2,1)} %get-tuple-element.14) | copy-start | bytes 3342340
  123.3 17.6 %all-to-all-start.5 = ((bf16[16,32,128]{2,1,0:T(8,128)(2,1)}), bf16[16,32,128]{2,1,0:T(8,128)(2,1)S(1)}, u32[]{:S(2)}, u32[]{:S(2)}) async-start(bf16[16,32,128]{2,1,0:T(8,128)(2,1)} %bitcast.42), calls=%async_computation.5 | async-start | bytes 262144 | tf_op jit(solution)/shard_map/all_to_all | solution.py:203
Sparse Core Ops, SparseCore 0:
  19.1 73.4 all-gather.5
  94.5 87.5 all-gather.3

commit v2 on v1

v2 whole, which is shorter than its diff:
```python
import functools

import jax
import jax.numpy as jnp
from jax import lax
from jax.experimental import pallas as pl
from jax.experimental.pallas import tpu as pltpu
from jax.sharding import PartitionSpec as P

HEAD_DIM = 64
BLOCK = 64
EDGE = 8
LANES = 128
EPS = 1.0
HIGH = lax.Precision.HIGHEST
F32 = jnp.float32
BF16 = jnp.bfloat16


def silu(v):
    return v / (1.0 + jnp.exp(-v))


def dot(a, b, contract=((1,), (0,))):
    return lax.dot_general(a, b, (contract, ((), ())), preferred_element_type=F32)


def taps_of(extended, taps_ref, count, length):
    first = EDGE - count + 1
    result = extended[first : first + length] * taps_ref[0:1]
    for k in range(1, count):
        result = result + extended[first + k : first + k + length] * taps_ref[k : k + 1]
    return result


def mixer_kernel(
    many, long_taps, short_taps, own_ref, recv_ref, rows_ref, taps_ref, taps_sc_ref, gain_ref, ab_ref, tail_ref, state_ref
):
    length = ab_ref.shape[1] - EDGE
    hd = HEAD_DIM

    @pl.when(pl.program_id(0) == 0)
    def _():
        tail_ref[...] = jnp.zeros_like(tail_ref)
        state_ref[...] = jnp.zeros_like(state_ref)

    lower = lax.broadcasted_iota(jnp.int32, (length, length), 0) >= lax.broadcasted_iota(
        jnp.int32, (length, length), 1
    )
    tail = tail_ref[...]
    state = state_ref[...]
    for k in range(many):
        rows = rows_ref[k]
        cols = rows.T
        step, cum, gate, gate_sc, inverse = (cols[:, i : i + 1] for i in range(5))
        stream = (own_ref[k] + recv_ref[k].astype(F32)) * inverse
        short_in = stream[:, 4 * hd : 5 * hd] * stream[:, 6 * hd : 7 * hd]
        conv = taps_of(jnp.concatenate([tail[:, : 4 * hd], stream[:, : 4 * hd]], axis=0), taps_ref, long_taps, length)
        conv_sc = taps_of(
            jnp.concatenate([tail[:, 4 * hd : 5 * hd], short_in], axis=0), taps_sc_ref, short_taps, length
        )
        tail = jnp.concatenate([stream[length - EDGE :, : 4 * hd], short_in[length - EDGE :], short_in[length - EDGE :]], axis=1)
        conv = silu(conv[:, : 3 * hd])
        x = conv[:, :hd] * step
        b = conv[:, hd : 2 * hd].astype(BF16)
        c = conv[:, 2 * hd : 3 * hd]
        z = stream[:, 3 * hd : 4 * hd]
        scb = stream[:, 5 * hd : 6 * hd]
        scores = dot(c.astype(BF16), b, ((1,), (1,)))
        decay = jnp.where(lower, jnp.exp(jnp.minimum(cum - rows[1:2], 0.0)), 0.0)
        core = dot((scores * decay).astype(BF16), x.astype(BF16))
        core = core + dot((c * jnp.exp(cum)).astype(BF16), state.astype(BF16), ((1,), (1,)))
        last = cum[length - 1 : length]
        fresh = dot((x * jnp.exp(last - cum)).astype(BF16), b, ((0,), (0,)))
        state = state * jnp.exp(last) + fresh
        gated = core * silu(z)
        squares = lax.dot_general(
            jnp.ones((EDGE, hd), F32), gated * gated, (((1,), (1,)), ((), ())), precision=HIGH, preferred_element_type=F32
        )
        coarse = squares.astype(BF16)
        fine = (squares - coarse.astype(F32)).astype(BF16)
        which = lax.broadcasted_iota(jnp.int32, squares.shape, 0)
        packed = jnp.where(which == 0, coarse.astype(F32), jnp.where(which == 1, fine.astype(F32), 0.0))
        both = jnp.concatenate([gated * gain_ref[...] * gate, gate_sc * (scb * conv_sc)], axis=1)
        ab_ref[k] = jnp.concatenate([both, packed], axis=0).astype(BF16)
    tail_ref[...] = tail
    state_ref[...] = state


def merge_kernel(per_group, ab_ref, out_ref):
    count, full = ab_ref.shape[0], ab_ref.shape[1]
    length = full - EDGE
    hd = HEAD_DIM
    ones = jnp.ones((per_group * EDGE, LANES), BF16)
    for g in range(count // per_group):
        squares = jnp.concatenate([ab_ref[g * per_group + k, length:, :] for k in range(per_group)], axis=0)
        mean = dot(squares, ones, ((0,), (0,))) * (1.0 / (per_group * hd))
        scale = lax.rsqrt(mean + EPS)[:, :hd]
        for k in range(0, per_group, 2):
            pair = []
            for j in range(2):
                ab = ab_ref[g * per_group + k + j, :length, :].astype(F32)
                pair.append(ab[:, :hd] * scale + ab[:, hd:])
            lo = (g * per_group + k) * hd
            out_ref[:, lo : lo + 2 * hd] = jnp.concatenate(pair, axis=1).astype(out_ref.dtype)


def gathered(x, axis):
    return lax.all_gather(x, axis)


def body(
    tokens,
    norm_gain,
    w_z,
    w_x,
    w_b,
    w_c,
    w_dt,
    w_gate,
    w_scb,
    w_scc,
    w_scx,
    conv_x,
    conv_b,
    conv_c,
    conv_sc,
    dt_bias,
    decay_log,
    group_gain,
    span_shift,
    w_out,
):
    sp, fs, tp = (lax.axis_size(a) for a in ("sp", "fs", "tp"))
    here, side = lax.axis_index("sp"), lax.axis_index("tp")
    own = tokens[0]
    length, half = own.shape
    hd = HEAD_DIM
    heads = dt_bias.shape[0]
    share = heads // sp
    groups = conv_b.shape[1] // hd
    per_group = heads // groups
    depth = w_x.shape[0]

    def cut(w):
        return jnp.moveaxis(w.reshape(w.shape[0], heads, hd), 1, 0)

    def cut_group(w):
        return jnp.repeat(jnp.moveaxis(w.reshape(w.shape[0], groups, hd), 1, 0), per_group, axis=0)

    packed = jnp.concatenate(
        [cut(w_x), cut_group(w_b), cut_group(w_c), cut(w_z), cut(w_scc), cut(w_scb), cut(w_scx)], axis=2
    )
    packed = jnp.pad(packed, ((0, 0), (0, 0), (0, hd)))
    cols = packed.shape[2]
    got = lax.all_to_all(packed, "sp", 0, 0, tiled=True)

    payload = jnp.concatenate([own, w_out], axis=0)
    everything = gathered(payload, "sp")

    halves = got.reshape(tp, (sp // tp) * depth, cols)
    halves = jnp.broadcast_to(halves, (fs, *halves.shape)).reshape(fs * tp, -1, cols)
    halves = lax.all_to_all(halves, ("fs", "tp"), 0, 0, tiled=True)
    weights = halves.reshape(fs, tp, sp // tp, depth, cols).transpose(1, 2, 0, 3, 4).reshape(tp, half, cols)
    gain = lax.dynamic_slice_in_dim(norm_gain, side * half, half)
    weights = (weights.astype(F32) * gain[:, None]).astype(BF16)
    w_mine = lax.dynamic_index_in_dim(weights, side, 0, keepdims=False)
    w_other = lax.dynamic_index_in_dim(weights, (tp - 1) - side, 0, keepdims=False)

    pair = lax.all_to_all(jnp.broadcast_to(own, (tp, *own.shape)), "tp", 0, 0, tiled=True)
    rows = jnp.concatenate([pair[k] for k in range(tp)], axis=1).astype(F32)
    inverse_rms = lax.rsqrt(jnp.mean(rows * rows, axis=1, keepdims=True) + EPS)
    normed = (rows * inverse_rms * norm_gain).astype(BF16)
    narrow = jnp.concatenate([w_dt, w_gate.reshape(w_gate.shape[0], -1)], axis=1)
    small = dot(narrow, normed, ((0,), (1,)))
    shift = jnp.repeat(span_shift[0], BLOCK)
    step = jax.nn.softplus(small[:heads] + dt_bias[:, None] + shift[None, :])
    rate = -jnp.exp(decay_log)[:, None]
    upper = (lax.iota(jnp.int32, length)[:, None] <= lax.iota(jnp.int32, length)[None, :]).astype(F32)
    cum = jnp.dot(step * rate, upper, precision=HIGH)
    gates = jax.nn.sigmoid(small[heads:])
    inverse_rows = jnp.broadcast_to(inverse_rms[:, 0][None, :], (heads, length))
    info = jnp.stack([step, cum, gates[:heads], gates[heads:], inverse_rows], axis=1)
    info = jnp.pad(info, ((0, 0), (0, EDGE - info.shape[1]), (0, 0)))
    info = lax.all_to_all(info, "sp", 0, 0, tiled=True)

    flat = everything.reshape(-1, half)
    other = dot(flat, w_other).astype(BF16)
    arrived = lax.ppermute(other, "tp", [(i, tp - 1 - i) for i in range(tp)])
    mine = dot(flat, w_mine)
    mine = mine.reshape(sp, -1, cols)
    arrived = arrived.reshape(sp, -1, cols)

    def head_of(a, dim):
        return lax.dynamic_slice_in_dim(a, here * share * hd, share * hd, dim)

    def group_of(a):
        return lax.dynamic_slice_in_dim(a, (here * share // per_group) * hd, hd, 1)

    taps = jnp.concatenate([head_of(conv_x, 1), group_of(conv_b), group_of(conv_c)], axis=1)
    taps = jnp.pad(taps, ((0, 0), (0, hd)))
    taps_sc = head_of(conv_sc, 1)
    own_gain = head_of(group_gain, 0)[None]
    many = 2
    block = lambda shape: pl.BlockSpec((many, *shape), lambda i: (i,) + (0,) * len(shape))
    whole = lambda a: pl.BlockSpec(a.shape, lambda i: (0,) * a.ndim)
    ab = pl.pallas_call(
        functools.partial(mixer_kernel, many, taps.shape[0], taps_sc.shape[0]),
        grid=(sp // many,),
        in_specs=[
            block((length, cols)),
            block((length, cols)),
            block((EDGE, length)),
            whole(taps),
            whole(taps_sc),
            whole(own_gain),
        ],
        out_specs=block((length + EDGE, 2 * hd)),
        out_shape=jax.ShapeDtypeStruct((sp, length + EDGE, 2 * hd), BF16),
        scratch_shapes=[pltpu.VMEM((EDGE, 6 * hd), F32), pltpu.VMEM((hd, hd), F32)],
        name="mixer",
    )(mine, arrived, info, taps, taps_sc, own_gain)

    w_rows = everything[:, length:].reshape(-1, half)
    w_all = lax.all_to_all(jnp.broadcast_to(w_rows, (fs, *w_rows.shape)), "fs", 0, 0, tiled=True)
    w_all = w_all.reshape(fs, sp, depth, half).transpose(1, 0, 2, 3).reshape(-1, half)

    ab = lax.all_to_all(ab, "sp", 0, 0, tiled=True)
    merged = pl.pallas_call(
        functools.partial(merge_kernel, per_group),
        out_shape=jax.ShapeDtypeStruct((length, sp * hd), BF16),
        name="merge",
    )(ab)
    partial = dot(merged, w_all, ((1,), (1,))).astype(BF16)
    parts = partial.reshape(tp, length // tp, partial.shape[1])
    parts = lax.all_to_all(parts, "tp", 0, 0, tiled=True)
    return parts.astype(F32).sum(axis=0).astype(BF16)[None]


def solution(mesh):
    return jax.shard_map(
        body,
        mesh=mesh,
        in_specs=(
            P(("grp", "fs"), "sp", "tp"),
            P(),
            P(("sp", "fs"), "tp"),
            P(("sp", "fs"), "tp"),
            P(("sp", "fs"), "tp"),
            P(("sp", "fs"), "tp"),
            P(None, "tp"),
            P(None, None, "tp"),
            P(("sp", "fs"), "tp"),
            P(("sp", "fs"), "tp"),
            P(("sp", "fs"), "tp"),
            P(None, "tp"),
            P(None, "tp"),
            P(None, "tp"),
            P(None, "tp"),
            P("tp"),
            P("tp"),
            P("tp"),
            P(("grp", "fs"), "sp"),
            P(("sp", "fs"), "tp"),
        ),
        out_specs=P(("grp", "fs"), ("sp", "tp"), None),
        check_vma=False,
    )
```

time: 235 us -> 241 us (1.026)
  blocking collectives: 106 us -> 10.9 us
  starting transfers between devices: 12.7 us -> 55.6 us
  waiting for transfers between devices: 54.8 us -> 94.6 us
  local copies, waits for them, and re-layouts: 19.6 us -> 28 us
  matrix products: 13.3 us -> 19 us
  Pallas kernels: 9.63 us -> 13.8 us
    all_to_all x2 -> x6, waiting for transfers between devices: 9.79 us -> 94.5 us  [the longest x1 31.2 us: body(): got = lax.all_to_all(packed, 'sp', 0, 0, tiled=True)]
    all_to_all x6 -> x1, blocking collectives: 93.3 us -> 10.9 us  [body(): parts = lax.all_to_all(parts, 'tp', 0, 0, tiled=True)]
    all_to_all x2 -> x6, starting transfers between devices: 8.03 us -> 53.3 us  [the longest x1 23.9 us: body(): lax.all_to_all(jnp.broadcast_to(own, (tp, *own.shape)), 'tp', 0, 0, tiled...]
    all_gather x2 -> x1, waiting for transfers between devices: 44.9 us -> 0.02 us  [gathered(): return lax.all_gather(x, axis)]
    all_gather x1 -> x0, blocking collectives: 13.1 us -> none  [body(): shifts = lax.all_gather(shift, 'fs')]
    dot_general x4, matrix products: 12.5 us -> 18.9 us  [dot(): lax.dot_general(a, b, (contract, ((), ())), preferred_element_type=F32)]
    broadcast_in_dim x2 -> x6, local copies, waits for them, and re-layouts: 1.48 us -> 7.21 us  [the longest x1 2.51 us: body(): jnp.broadcast_to(w_rows, (fs, *w_rows.shape))]
    transpose x0 -> x1, local copies, waits for them, and re-layouts: none -> 4.94 us  [body(): w_all.reshape(fs, sp, depth, half).transpose(1, 0, 2, 3).reshape(-1, half)]
  transfers between devices with their start and end apart: 5 -> 8, of which waited for: 3 -> 5; matrix products, arithmetic and copies ran while one was open for 10% -> 17% of each run, Pallas kernels for 2% -> 5%
where the time goes in v2:
time: 241 us; the launch traced here: 240 us
  waiting for transfers between devices  94.6 us (39%)
  starting transfers between devices  55.6 us (23%)
  local copies, waits for them, and re-layouts  28 us (12%)
  matrix products  19 us (8%)
  Pallas kernels  13.8 us (6%)
  between operations  13.7 us (6%)
  blocking collectives  10.9 us (5%)
  other arithmetic  4.45 us (2%)
    all_to_all x1, waiting for transfers between devices, body(): got = lax.all_to_all(packed, 'sp', 0, 0, tiled=True)  31.2 us
    all_to_all x1, waiting for transfers between devices, body(): halves = lax.all_to_all(halves, ('fs', 'tp'), 0, 0, tiled=True)  24.5 us
    all_to_all x1, starting transfers between devices, body(): lax.all_to_all(jnp.broadcast_to(own, (tp, *own.shape)), 'tp', 0, 0, tiled...  23.9 us
    dot_general x4, matrix products, dot(): lax.dot_general(a, b, (contract, ((), ())), preferred_element_type=F32)  18.9 us
    all_to_all x1, waiting for transfers between devices, body(): ab = lax.all_to_all(ab, 'sp', 0, 0, tiled=True)  18.1 us
    all_to_all x1, waiting for transfers between devices, body(): lax.all_to_all(jnp.broadcast_to(w_rows, (fs, *w_rows.shape)), 'fs', 0, 0,...  13.1 us
    pallas_call x1, Pallas kernels, body(): pl.pallas_call(functools.partial(mixer_kernel, many, taps.shape[0], taps_...  11.6 us
    all_to_all x1, blocking collectives, body(): parts = lax.all_to_all(parts, 'tp', 0, 0, tiled=True)  10.9 us
  transfers between devices with their start and end apart: 8, of which 5 were waited for; matrix products, arithmetic and copies ran while one was open for 17% of the time, Pallas kernels for 5%

profile of v2, /device:TPU:33, one launch (start us, length us, event | category | flops | bytes accessed | tf_op | source)
XLA Modules:
  0.0 240.1 jit_solution(8275530136050782923)
XLA Ops:
  6.5 0.0 copy-start
  6.6 1.7 pad_maximum_fusion.2
  8.3 0.1 all-gather.3.cloned.1.call-update
  8.4 1.8 broadcast_in_dim.33
  10.2 23.9 %all-to-all-start.2 = ((bf16[2,128,1024]{2,1,0:T(8,128)(2,1)}), bf16[2,128,1024]{2,1,0:T(8,128)(2,1)S(1)}, u32[]{:S(2)}, u32[]{:S(2)}) async-start(bf16[2,128,1024]{2,1,0:T(8,128)(2,1)} %broadcast_in_dim.33), calls=%async_computation.2 | async-start | bytes 1048576 | tf_op jit(solution)/shard_map/all_to_all | solution.py:170
  34.1 0.8 reshape.86
  34.9 0.8 reshape.88
  35.7 1.0 reshape.93
  36.7 1.0 reshape.85
  37.7 1.0 reshape.90
  38.7 1.0 reshape.91
  39.7 1.0 reshape.92
  40.8 0.4 concatenate.16
  41.3 0.3 copy.37
  41.6 0.9 pad.12.clone
  42.4 0.0 all-to-all-done.2
  42.4 4.7 %all-to-all-start = ((bf16[16,32,512]{2,1,0:T(8,128)(2,1)}), bf16[16,32,512]{2,1,0:T(8,128)(2,1)S(1)}, u32[]{:S(2)}, u32[]{:S(2)}) async-start(bf16[16,32,512]{2,1,0:T(8,128)(2,1)} %pad.12.clone), calls=%async_computation | async-start | bytes 1048576 | tf_op jit(solution)/shard_map/all_to_all | solution.py:156
  47.2 0.1 broadcast_in_dim.34
  47.3 0.1 add.74
  47.3 31.2 %all-to-all-done = bf16[16,32,512]{2,1,0:T(8,128)(2,1)S(1)} async-done(((bf16[16,32,512]{2,1,0:T(8,128)(2,1)}), bf16[16,32,512]{2,1,0:T(8,128)(2,1)S(1)}, u32[]{:S(2)}, u32[]{:S(2)}) %all-to-all-start) | async-done | bytes 524320 | tf_op jit(solution)/shard_map/all_to_all | solution.py:156
  78.5 1.5 broadcast_in_dim.32
  80.1 7.7 %all-to-all-start.1 = ((bf16[8,256,512]{2,1,0:T(8,128)(2,1)}), bf16[8,256,512]{2,1,0:T(8,128)(2,1)S(1)}, u32[]{:S(2)}, u32[]{:S(2)}) async-start(bf16[8,256,512]{2,1,0:T(8,128)(2,1)} %bitcast.56), calls=%async_computation.1 | async-start | bytes 4194304 | tf_op jit(solution)/shard_map/all_to_all | solution.py:163
  87.8 0.2 fusion.1
  88.0 0.0 copy-done.5
  88.0 0.0 copy-done.9
  88.0 0.4 fusion.9
  88.4 0.0 copy-done.8
  88.4 0.1 compare_select_fusion
  88.5 0.2 fusion.16
  88.7 0.1 stack.19
  88.8 0.6 pad.13
  89.5 24.5 %all-to-all-done.1 = bf16[8,256,512]{2,1,0:T(8,128)(2,1)S(1)} async-done(((bf16[8,256,512]{2,1,0:T(8,128)(2,1)}), bf16[8,256,512]{2,1,0:T(8,128)(2,1)S(1)}, u32[]{:S(2)}, u32[]{:S(2)}) %all-to-all-start.1) | async-done | bytes 2097184 | tf_op jit(solution)/shard_map/all_to_all | solution.py:163
  113.9 7.5 %all-to-all-start.3 = ((f32[16,8,128]{2,1,0:T(8,128)}), f32[16,8,128]{2,1,0:T(8,128)S(1)}, u32[]{:S(2)}, u32[]{:S(2)}) async-start(f32[16,8,128]{2,1,0:T(8,128)} %pad.13), calls=%async_computation.3 | async-start | bytes 131072 | tf_op jit(solution)/shard_map/all_to_all | solution.py:185
  121.4 0.6 convert_bitcast_fusion
  122.0 0.0 dynamic-slice-start
  122.0 0.8 copy.34
  122.9 0.3 fusion
  123.2 0.0 all-gather.3.cloned.1.call-done
  123.2 2.1 slice.34
  125.3 7.7 %all-to-all-done.3.rows_ref = f32[16,8,128]{2,1,0:T(8,128)S(1)} async-done(((f32[16,8,128]{2,1,0:T(8,128)}), f32[16,8,128]{2,1,0:T(8,128)S(1)}, u32[]{:S(2)}, u32[]{:S(2)}) %all-to-all-start.3) | async-done | bytes 65568 | tf_op jit(solution)/shard_map/all_to_all | solution.py:185
  132.9 2.5 %broadcast_in_dim.36 = bf16[4,512,1024]{2,1,0:T(8,128)(2,1)} broadcast(bf16[512,1024]{1,0:T(8,128)(2,1)S(1)} %bitcast.57), dimensions={1,2} | broadcast | bytes 5242880 | tf_op jit(solution)/shard_map/broadcast_in_dim | solution.py:225
  135.4 4.9 %all-to-all-start.5 = ((bf16[4,512,1024]{2,1,0:T(8,128)(2,1)}), bf16[4,512,1024]{2,1,0:T(8,128)(2,1)}, u32[]{:S(2)}, u32[]{:S(2)}) async-start(bf16[4,512,1024]{2,1,0:T(8,128)(2,1)} %broadcast_in_dim.36), calls=%async_computation.5 | async-start | bytes 8388608 | tf_op jit(solution)/shard_map/all_to_all | solution.py:225
  140.4 0.0 copy-start.6
  140.4 0.0 copy-start.7
  140.4 6.7 %convolution_convert_fusion = bf16[2560,512]{1,0:T(8,128)(2,1)} fusion(bf16[2560,1024]{1,0:T(8,128)(2,1)} %all-gather.3.cloned.1.call-done, bf16[2,1024,512]{2,1,0:T(8,128)(2,1)S(1)} %fusion, s32[]{:T(128)S(6)} %select_n.31), kind=kOutput, calls=%fused_computation | convolution fusion | flops 2685665280 | bytes 8912900 | tf_op jit(solution)/shard_map/dot_general | solution.py:25
  147.1 2.3 collective-permute-start
  149.4 1.3 dynamic-slice_bitcast_fusion.gain_ref
  150.7 0.1 constant_dynamic-slice_fusion.3
  150.7 1.3 constant_dynamic-slice_fusion.taps_sc_ref
  152.1 0.1 constant_dynamic-slice_fusion.1
  152.2 0.7 select_maximum_fusion.taps_ref
  152.8 8.0 %fusion.5.own_ref = f32[16,160,512]{2,1,0:T(8,128)} fusion(bf16[16,160,1024]{2,1,0:T(8,128)(2,1)} %bitcast.71, bf16[2,1024,512]{2,1,0:T(8,128)(2,1)} %copy-done.3, s32[]{:T(128)S(6)} %select_n.30), kind=kOutput, calls=%fused_computation.11 | convolution fusion | flops 2684354560 | bytes 11534340 | tf_op jit(solution)/shard_map/dot_general | solution.py:25
  160.9 0.0 collective-permute-done
  160.9 1.5 copy-done.1
  162.4 11.6 %mixer.1 = bf16[16,136,128]{2,1,0:T(8,128)(2,1)} custom-call(f32[16,160,512]{2,1,0:T(8,128)} %fusion.5.own_ref, bf16[16,160,512]{2,1,0:T(8,128)(2,1)} %bitcast.58, f32[16,8,128]{2,1,0:T(8,128)} %copy-done.4, f32[4,256]{1,0:T(4,128)} %select_maximum_fusion.taps_ref, f32[3,64]{1,0:T(4,128)} %constant_dynamic-slice_fusion.taps_sc_ref, ...), custom_call_target="tpu_custom_call" | custom-call | tf_op jit(solution)/shard_map/mixer/pallas_call | solution.py:207
  173.9 13.1 %all-to-all-done.5 = bf16[4,512,1024]{2,1,0:T(8,128)(2,1)} async-done(((bf16[4,512,1024]{2,1,0:T(8,128)(2,1)}), bf16[4,512,1024]{2,1,0:T(8,128)(2,1)}, u32[]{:S(2)}, u32[]{:S(2)}) %all-to-all-start.5) | async-done | bytes 4194336 | tf_op jit(solution)/shard_map/all_to_all | solution.py:225
  187.0 4.6 %all-to-all-start.4 = ((bf16[16,136,128]{2,1,0:T(8,128)(2,1)}), bf16[16,136,128]{2,1,0:T(8,128)(2,1)S(1)}, u32[]{:S(2)}, u32[]{:S(2)}) async-start(bf16[16,136,128]{2,1,0:T(8,128)(2,1)} %mixer.1), calls=%async_computation.4 | async-start | bytes 1114112 | tf_op jit(solution)/shard_map/all_to_all | solution.py:228
  191.6 4.9 %copy.36 = bf16[16,4,32,1024]{3,2,1,0:T(8,128)(2,1)} copy(bf16[16,4,32,1024]{3,2,0,1:T(8,128)(2,1)} %bitcast.32) | data formatting | bytes 8388608 | tf_op jit(solution)/shard_map/transpose | solution.py:226
  196.5 18.1 %all-to-all-done.4.ab_ref = bf16[16,136,128]{2,1,0:T(8,128)(2,1)S(1)} async-done(((bf16[16,136,128]{2,1,0:T(8,128)(2,1)}), bf16[16,136,128]{2,1,0:T(8,128)(2,1)S(1)}, u32[]{:S(2)}, u32[]{:S(2)}) %all-to-all-start.4) | async-done | bytes 557088 | tf_op jit(solution)/shard_map/all_to_all | solution.py:228
  214.6 0.8 copy-done.2
  215.4 2.3 merge.1
  217.7 3.8 %convolution_convert_fusion.1 = bf16[128,2048]{1,0:T(8,128)(2,1)S(1)} fusion(bf16[128,1024]{1,0:T(8,128)(2,1)} %merge.1, bf16[2048,1024]{1,0:T(8,128)(2,1)} %bitcast.54), kind=kOutput, calls=%fused_computation.4 | convolution fusion | flops 537133056 | bytes 4980736 | tf_op jit(solution)/shard_map/dot_general | solution.py:25
  221.5 10.9 %all_to_all.35 = bf16[2,64,2048]{2,1,0:T(8,128)(2,1)S(1)} all-to-all(bf16[2,64,2048]{2,1,0:T(8,128)(2,1)S(1)} %bitcast.60), channel_id=1, replica_groups=mesh['grp'=2,'sp'=16,'fs'=4,'tp'=2] {'tp'}, dimensions={0} | all-to-all | bytes 1048576 | tf_op jit(solution)/shard_map/all_to_all | solution.py:236
  232.4 0.8 reduce_sum.22
  (28 shorter events, 0.2 us)
Async XLA Ops:
  6.5 144.1 %copy-start = (f32[4,1024]{1,0:T(4,128)S(1)}, f32[4,1024]{1,0:T(4,128)}, u32[]{:S(2)}) copy-start(f32[4,1024]{1,0:T(4,128)} %param.31) | copy-start | bytes 49156
  6.6 116.6 %all-gather.3.cloned.1.call-start = ((), (), s32[]{:S(2)}) async-start(), calls=%async_computation.7 | async-start | bytes 5570560 | tf_op jit(solution)/shard_map/all_gather | solution.py:109
  8.3 38.9 %copy-start.11 = (f32[1,2]{1,0:T(1,128)S(1)}, f32[1,2]{1,0:T(1,128)}, u32[]{:S(2)}) copy-start(f32[1,2]{1,0:T(1,128)} %param.38) | copy-start | bytes 28
  10.2 32.2 %all-to-all-start.2 = ((bf16[2,128,1024]{2,1,0:T(8,128)(2,1)}), bf16[2,128,1024]{2,1,0:T(8,128)(2,1)S(1)}, u32[]{:S(2)}, u32[]{:S(2)}) async-start(bf16[2,128,1024]{2,1,0:T(8,128)(2,1)} %broadcast_in_dim.33), calls=%async_computation.2 | async-start | bytes 1048576 | tf_op jit(solution)/shard_map/all_to_all | solution.py:170
  42.4 36.1 %all-to-all-start = ((bf16[16,32,512]{2,1,0:T(8,128)(2,1)}), bf16[16,32,512]{2,1,0:T(8,128)(2,1)S(1)}, u32[]{:S(2)}, u32[]{:S(2)}) async-start(bf16[16,32,512]{2,1,0:T(8,128)(2,1)} %pad.12.clone), calls=%async_computation | async-start | bytes 1048576 | tf_op jit(solution)/shard_map/all_to_all | solution.py:156
  78.5 9.4 %copy-start.12 = (f32[16]{0:T(128)S(1)}, f32[16]{0:T(128)}, u32[]{:S(2)}) copy-start(f32[16]{0:T(128)} %param.36) | copy-start | bytes 196
  78.5 9.4 %copy-start.5 = (f32[2048]{0:T(1024)S(1)}, f32[2048]{0:T(1024)}, u32[]{:S(2)}) copy-start(f32[2048]{0:T(1024)} %param.21) | copy-start | bytes 24580
  78.5 9.5 %copy-start.9 = (bf16[2048,2,16]{0,2,1:T(8,128)(2,1)S(1)}, bf16[2048,2,16]{0,2,1:T(8,128)(2,1)}, u32[]{:S(2)}) copy-start(bf16[2048,2,16]{0,2,1:T(8,128)(2,1)} %param.27) | copy-start | bytes 393220
  78.5 9.5 %copy-start.10 = (bf16[2048,16]{0,1:T(8,128)(2,1)S(1)}, bf16[2048,16]{0,1:T(8,128)(2,1)}, u32[]{:S(2)}) copy-start(bf16[2048,16]{0,1:T(8,128)(2,1)} %param.26) | copy-start | bytes 196612
  80.1 8.3 %copy-start.8 = (f32[16]{0:T(128)S(1)}, f32[16]{0:T(128)}, u32[]{:S(2)}) copy-start(f32[16]{0:T(128)} %param.35) | copy-start | bytes 196
  80.1 33.9 %all-to-all-start.1 = ((bf16[8,256,512]{2,1,0:T(8,128)(2,1)}), bf16[8,256,512]{2,1,0:T(8,128)(2,1)S(1)}, u32[]{:S(2)}, u32[]{:S(2)}) async-start(bf16[8,256,512]{2,1,0:T(8,128)(2,1)} %bitcast.56), calls=%async_computation.1 | async-start | bytes 4194304 | tf_op jit(solution)/shard_map/all_to_all | solution.py:163
  113.9 19.0 %all-to-all-start.3 = ((f32[16,8,128]{2,1,0:T(8,128)}), f32[16,8,128]{2,1,0:T(8,128)S(1)}, u32[]{:S(2)}, u32[]{:S(2)}) async-start(f32[16,8,128]{2,1,0:T(8,128)} %pad.13), calls=%async_computation.3 | async-start | bytes 131072 | tf_op jit(solution)/shard_map/all_to_all | solution.py:185
  122.0 0.8 dynamic-slice-start
  123.2 17.2 %copy-start.3 = (bf16[2,1024,512]{2,1,0:T(8,128)(2,1)}, bf16[2,1024,512]{2,1,0:T(8,128)(2,1)S(1)}, u32[]{:S(2)}) copy-start(bf16[2,1024,512]{2,1,0:T(8,128)(2,1)S(1)} %fusion) | copy-start | bytes 6291460
  132.9 2.5 %copy-start.4 = (f32[16,8,128]{2,1,0:T(8,128)}, f32[16,8,128]{2,1,0:T(8,128)S(1)}, u32[]{:S(2)}) copy-start(f32[16,8,128]{2,1,0:T(8,128)S(1)} %all-to-all-done.3.rows_ref) | copy-start | bytes 196612
  135.4 51.5 %all-to-all-start.5 = ((bf16[4,512,1024]{2,1,0:T(8,128)(2,1)}), bf16[4,512,1024]{2,1,0:T(8,128)(2,1)}, u32[]{:S(2)}, u32[]{:S(2)}) async-start(bf16[4,512,1024]{2,1,0:T(8,128)(2,1)} %broadcast_in_dim.36), calls=%async_computation.5 | async-start | bytes 8388608 | tf_op jit(solution)/shard_map/all_to_all | solution.py:225
  140.4 11.7 %copy-start.6 = (f32[4,256]{1,0:T(4,128)S(1)}, f32[4,256]{1,0:T(4,128)}, u32[]{:S(2)}) copy-start(f32[4,256]{1,0:T(4,128)} %param.33) | copy-start | bytes 12292
  140.4 11.7 %copy-start.7 = (f32[4,256]{1,0:T(4,128)S(1)}, f32[4,256]{1,0:T(4,128)}, u32[]{:S(2)}) copy-start(f32[4,256]{1,0:T(4,128)} %param.32) | copy-start | bytes 12292
  147.1 13.8 %collective-permute-start = (bf16[2560,512]{1,0:T(8,128)(2,1)}, bf16[2560,512]{1,0:T(8,128)(2,1)S(1)}, u32[]{:S(2)}, u32[]{:S(2)}) collective-permute-start(bf16[2560,512]{1,0:T(8,128)(2,1)} %convolution_convert_fusion), channel_id=1, source_target_pairs={{0,1},{1,0},{2,3},{3,2},{4,5},{5,4},{6,7},{7,6},{8,9},{9,8},{10,11... | collective-permute-start | bytes 7864328 | tf_op jit(solution)/shard_map/ppermute | solution.py:189
  160.9 1.5 copy-start.1
  187.0 27.6 %all-to-all-start.4 = ((bf16[16,136,128]{2,1,0:T(8,128)(2,1)}), bf16[16,136,128]{2,1,0:T(8,128)(2,1)S(1)}, u32[]{:S(2)}, u32[]{:S(2)}) async-start(bf16[16,136,128]{2,1,0:T(8,128)(2,1)} %mixer.1), calls=%async_computation.4 | async-start | bytes 1114112 | tf_op jit(solution)/shard_map/all_to_all | solution.py:228
  214.6 0.8 copy-start.2
Sparse Core Ops, SparseCore 0:
  9.1 108.6 all-gather.2
